TPU v7x, 256 devices: a whole 4x4x8 slice. The times are simulated.
256 devices in a mesh: ep: 64 (over z, y, core), tp: 4 (over x).
Axes of the slice: x: 4, y: 4, z: 8, core: 2. Of those that a mesh axis runs over, the one named last changes fastest.
Arguments:
- mixer_in: bfloat16 [32768, 2048], P('ep'), may hold values from -6 to 6
- mixer_gain: float32 [2048], replicated, may hold values from 0.1 to 1.9
- query_weight: bfloat16 [2048, 1024], P(None, 'tp'), may hold values from -0.125 to 0.125
- key_weight: bfloat16 [2048, 1024], P(None, 'tp'), may hold values from -0.125 to 0.125
- value_weight: bfloat16 [2048, 1024], P(None, 'tp'), may hold values from -0.125 to 0.125
- input_gate: float32 [8, 32768], P('tp', 'ep'), may hold values from -4 to 240
- forget_gate: float32 [8, 32768], P('tp', 'ep'), may hold values from 0 to 25
- head_gain: float32 [1024], replicated, may hold values from 0.1 to 1.9
- mixer_out_weight: bfloat16 [1024, 2048], P('tp'), may hold values from -0.1875 to 0.1875
- expert_in: bfloat16 [16384, 2048], P('ep'), may hold values from -6 to 6
- expert_gain: float32 [2048], replicated, may hold values from 0.1 to 1.9
- group_router: bfloat16 [2048, 16], replicated, may hold values from -0.125 to 0.125
- expert_router: bfloat16 [2048, 64], replicated, may hold values from -0.125 to 0.125
- routes: int32 [16384, 2], P('ep'), may hold values from 0 to 63, all different within a row; in each aligned block of 256 rows (0 to 255, 256 to 511, ...) at most 16 rows name the same one
- gate_experts: bfloat16 [64, 2048, 1024], P('ep', None, 'tp'), may hold values from -0.125 to 0.125
- up_experts: bfloat16 [64, 2048, 1024], P('ep', None, 'tp'), may hold values from -0.125 to 0.125
- down_experts: bfloat16 [64, 1024, 2048], P('ep', 'tp'), may hold values from -0.1875 to 0.1875
Outputs:
- mixer_out: bfloat16 [32768, 2048], P(('ep', 'tp'))
- expert_out: bfloat16 [16384, 2048], P('ep', 'tp')
Inputs may be any that keep to these rules, and one draw needn't show every extreme that they name: `routes`: each row names 2 different experts. In each aligned block of 256 rows (the rows of one index of ep) no expert is named by more than 16 rows, a bound that some block reaches.
All inputs are finite; a program needn't handle non-finite values.
Results may differ from a plain program's by a relative error of at most 0.014.
The roundings to bfloat16 on the way count: a program that leaves them out, or rounds other values in their place, can miss the bound.
Values may be sent and summed in bfloat16 or wider, within the bound.
A program may use at most 128 MiB of HBM per device.

v0:
```python
import jax
import jax.numpy as jnp
from jax import lax
from jax.sharding import Mesh
from jax.sharding import PartitionSpec as P

BLOCK = 128
EP = ("ep_0", "ep_1", "ep_2")
EP_TP = ("ep_0", "ep_1", "ep_2", "tp")


epsilon = 1e-06
highest = lax.Precision.HIGHEST
floor_log = -1e30


def filled_with(x, identity):
    return jax.tree.map(
        lambda a, e: jnp.broadcast_to(jnp.asarray(e, a.dtype), a.shape), x, identity
    )


def collected_together(x, axis):
    leaves = jax.tree.leaves(x)
    order = sorted(range(len(leaves)), key=lambda k: -leaves[k].size)
    width = (1, *leaves[order[0]].shape)[-1]
    lines = [
        jnp.pad(leaves[k].reshape(-1), (0, -leaves[k].size % width)).reshape(-1, width)
        for k in order
    ]
    both, at, found = (lax.all_gather(jnp.concatenate(lines), axis), 0, {})
    for k, line in zip(order, lines):
        slab = both[:, at : at + len(line)].reshape(len(both), -1)
        found[k] = slab[:, : leaves[k].size].reshape(-1, *leaves[k].shape)
        at += len(line)
    numbers = iter(range(len(leaves)))
    return jax.tree.map(lambda _: found[next(numbers)], x)


def prefix_by_axis(x, axes, combine, identity):
    before = start = filled_with(x, identity)
    so_far = x
    for axis in reversed(axes):
        length, place = (lax.axis_size(axis), lax.axis_index(axis))
        pieces = collected_together(so_far, axis)
        inside, so_far = (start, start)
        for k in range(length):
            passed = k < place
            so_far = combine(so_far, jax.tree.map(lambda part: part[k], pieces))
            inside = jax.tree.map(lambda new, old: jnp.where(passed, new, old), so_far, inside)
        before = combine(inside, before)
    return before


def split_up(x, dim, length):
    shape = x.shape
    parts = x.reshape(*shape[:dim], length, shape[dim] // length, *shape[dim + 1 :])
    return jnp.moveaxis(parts, dim, 0)


def sum_at_owner(x, axis, dim):
    length = lax.axis_size(axis)
    parts = lax.all_to_all(split_up(x, dim, length), axis, 0, 0, tiled=True)
    return jnp.sum(parts.astype(jnp.float32), axis=0)


def rms_rows(matrix, gain):
    widened = matrix.astype(jnp.float32)
    scaled = widened * lax.rsqrt(jnp.mean(widened * widened, axis=-1, keepdims=True) + epsilon)
    return scaled * gain


def block_state(keys, value_rows, input_block, forget_block, scale):
    cumulative = jnp.cumsum(forget_block, axis=-1)
    total_log = cumulative[..., -1]
    log_weight = total_log[..., None] - cumulative + input_block
    peak_log = jnp.max(log_weight, axis=-1)
    weights = jnp.exp(log_weight - peak_log[..., None])
    key_float = keys.astype(jnp.float32) * scale
    value_weighted = value_rows.astype(jnp.float32) * weights[..., None]
    memory = jnp.einsum("...sv,...sk->...vk", value_weighted, key_float, precision=highest)
    return (memory, peak_log, total_log)


def merge_state(earlier, later):
    peak_log = jnp.maximum(later[2] + earlier[1], later[1])
    fade_earlier = jnp.exp(later[2] + earlier[1] - peak_log)
    fade_later = jnp.exp(later[1] - peak_log)
    memory = fade_earlier[..., None, None] * earlier[0] + fade_later[..., None, None] * later[0]
    return (memory, peak_log, earlier[2] + later[2])


def block_out(queries, keys, value_rows, input_block, forget_block, state, scale):
    cumulative = jnp.cumsum(forget_block, axis=-1)
    length = cumulative.shape[-1]
    causal = jnp.tril(jnp.ones((length, length), dtype=bool))
    within = jnp.where(
        causal,
        cumulative[..., :, None] - cumulative[..., None, :] + input_block[..., None, :],
        -jnp.inf,
    )
    carried = cumulative + state[1][..., None]
    highest_log = jnp.maximum(jnp.max(within, axis=-1), carried)
    weight_within = jnp.exp(within - highest_log[..., None])
    weight_carried = jnp.exp(carried - highest_log)
    raw_scores = (
        jnp.einsum("...td,...sd->...ts", queries, keys, preferred_element_type=jnp.float32) * scale
    )
    block_scores = raw_scores * weight_within
    numerator = jnp.einsum(
        "...ts,...sd->...td",
        block_scores.astype(jnp.bfloat16),
        value_rows,
        preferred_element_type=jnp.float32,
    )
    query_float = queries.astype(jnp.float32)
    return numerator + weight_carried[..., None] * jnp.einsum(
        "...vk,...tk->...tv", state[0], query_float, precision=highest
    )


def take_block(states, block_index):
    return tuple((member[block_index] for member in states))


def route_weights(group_logits, expert_logits, routes):
    members = expert_logits.shape[1] // group_logits.shape[1]
    chosen = jnp.take_along_axis(expert_logits, routes, axis=1)
    group_pick = jnp.take_along_axis(group_logits, routes // members, axis=1)
    return jax.nn.sigmoid(group_pick) * jax.nn.sigmoid(chosen - chosen[:, ::-1])


def shards(
    mixer_in,
    mixer_gain,
    query_weight,
    key_weight,
    value_weight,
    input_gate,
    forget_gate,
    head_gain,
    mixer_out_weight,
    expert_in,
    expert_gain,
    group_router,
    expert_router,
    routes,
    gate_experts,
    up_experts,
    down_experts,
):
    normed_a = rms_rows(mixer_in, mixer_gain).astype(jnp.bfloat16)
    queries = jnp.dot(normed_a, query_weight, preferred_element_type=jnp.float32).astype(
        jnp.bfloat16
    )
    keys = jnp.dot(normed_a, key_weight, preferred_element_type=jnp.float32).astype(jnp.bfloat16)
    value_rows = jnp.dot(normed_a, value_weight, preferred_element_type=jnp.float32).astype(
        jnp.bfloat16
    )
    row_count = normed_a.shape[0]
    head_local = input_gate.shape[0]
    width_local = queries.shape[1]
    head_size = width_local // head_local
    block_count = row_count // BLOCK
    scale = head_size ** (-0.5)

    def split_heads(matrix):
        return matrix.reshape(block_count, BLOCK, head_local, head_size).transpose(0, 2, 1, 3)

    def split_gates(gates):
        return gates.reshape(head_local, block_count, BLOCK).transpose(1, 0, 2)

    query_blocks = split_heads(queries)
    key_blocks = split_heads(keys)
    value_blocks = split_heads(value_rows)
    input_blocks = split_gates(input_gate)
    forget_blocks = split_gates(jax.nn.log_sigmoid(forget_gate))
    summaries = block_state(key_blocks, value_blocks, input_blocks, forget_blocks, scale)
    summary = take_block(summaries, 0)
    for block_index in range(1, block_count):
        summary = merge_state(summary, take_block(summaries, block_index))
    identity = (
        jnp.zeros_like(summary[0]),
        jnp.full_like(summary[1], floor_log),
        jnp.zeros_like(summary[2]),
    )
    current = prefix_by_axis(summary, EP, merge_state, identity)
    start_list = [current]
    for block_index in range(block_count - 1):
        current = merge_state(current, take_block(summaries, block_index))
        start_list.append(current)
    starts = tuple((jnp.stack([entry[member] for entry in start_list]) for member in range(3)))
    cells = block_out(
        query_blocks, key_blocks, value_blocks, input_blocks, forget_blocks, starts, scale
    )
    cells = cells.transpose(0, 2, 1, 3).reshape(row_count, head_local, head_size)
    gain_local = lax.dynamic_slice_in_dim(
        head_gain, lax.axis_index("tp") * width_local, width_local
    ).reshape(head_local, head_size)
    cell_rows = rms_rows(cells, gain_local).reshape(row_count, width_local).astype(jnp.bfloat16)
    mixer_out = sum_at_owner(
        jnp.dot(cell_rows, mixer_out_weight, preferred_element_type=jnp.float32).astype(
            jnp.bfloat16
        ),
        "tp",
        0,
    ).astype(jnp.bfloat16)
    normed_b = rms_rows(expert_in, expert_gain).astype(jnp.bfloat16)
    group_logits = jnp.dot(normed_b, group_router, preferred_element_type=jnp.float32)
    expert_logits = jnp.dot(normed_b, expert_router, preferred_element_type=jnp.float32)
    combine = route_weights(group_logits, expert_logits, routes)
    token_count = normed_b.shape[0]
    expert_total = expert_logits.shape[1]
    capacity = 4 * token_count // expert_total
    flat_routes = routes.reshape(-1)
    pair_total = flat_routes.shape[0]
    matches = (flat_routes[:, None] == jnp.arange(expert_total, dtype=jnp.int32)[None, :]).astype(
        jnp.int32
    )
    sequence_place = jnp.sum(jnp.cumsum(matches, axis=0) * matches, axis=1) - 1
    slot_index = flat_routes * capacity + sequence_place
    owner = (
        jnp.full((expert_total * capacity,), pair_total, jnp.int32)
        .at[slot_index]
        .set(jnp.arange(pair_total, dtype=jnp.int32))
    )
    padded = jnp.concatenate([normed_b, jnp.zeros((1, normed_b.shape[1]), jnp.bfloat16)], axis=0)
    outgoing = padded[owner // 2].reshape(expert_total, capacity, normed_b.shape[1])
    gate_weight = gate_experts[0]
    up_weight = up_experts[0]
    down_weight = down_experts[0]
    arrived = lax.all_to_all(outgoing, EP, split_axis=0, concat_axis=0, tiled=True)
    gate_act = jnp.einsum("scd,df->scf", arrived, gate_weight, preferred_element_type=jnp.float32)
    up_act = jnp.einsum("scd,df->scf", arrived, up_weight, preferred_element_type=jnp.float32)
    hidden = (jax.nn.silu(gate_act) * up_act).astype(jnp.bfloat16)
    partial_rows = jnp.einsum(
        "scf,fo->sco", hidden, down_weight, preferred_element_type=jnp.float32
    )
    summed = lax.psum_scatter(
        partial_rows.astype(jnp.bfloat16), "tp", scatter_dimension=2, tiled=True
    )
    returned = lax.all_to_all(summed, EP, split_axis=0, concat_axis=0, tiled=True)
    picked = jnp.take(returned.reshape(-1, returned.shape[2]), slot_index, axis=0).astype(
        jnp.float32
    )
    weighted = picked * combine.reshape(-1)[:, None]
    expert_out = jnp.sum(weighted.reshape(token_count, 2, weighted.shape[1]), axis=1).astype(
        jnp.bfloat16
    )
    return (mixer_out, expert_out)


def solution(mesh):
    split = Mesh(mesh.devices.reshape(8, 4, 2, mesh.shape["tp"]), ("ep_0", "ep_1", "ep_2", "tp"))
    placed = (
        P(EP, None),
        P(),
        P(None, "tp"),
        P(None, "tp"),
        P(None, "tp"),
        P("tp", EP),
        P("tp", EP),
        P(),
        P("tp", None),
        P(EP, None),
        P(),
        P(),
        P(),
        P(EP, None),
        P(EP, None, "tp"),
        P(EP, None, "tp"),
        P(EP, "tp", None),
    )
    return jax.shard_map(
        shards,
        mesh=split,
        in_specs=placed,
        out_specs=(P(EP_TP, None), P(EP, "tp")),
        check_vma=False,
    )
```

profile of v0, /device:TPU:1, one launch (start us, length us, event | category | flops | bytes accessed | tf_op | source)
XLA Modules:
  0.0 275.8 jit_solution(7234844089155936487)
XLA Ops:
  9.9 1.5 fusion.3
  13.4 2.4 scatter_custom_fusion
  15.9 1.5 fusion.5
  17.5 6.0 %gather_fusion = bf16[1024,2048]{1,0:T(8,128)(2,1)} fusion(bf16[257,2048]{1,0:T(8,128)(2,1)S(1)} %concatenate.15, s32[1024]{0:T(1024)S(1)} %fusion.84), kind=kCustom, calls=%fused_computation | custom fusion | bytes 8392704 | tf_op jit(solution)/shard_map/gather | solution.py:228
  23.5 13.5 %all-to-all-start.1 = ((bf16[64,16,2048]{2,1,0:T(8,128)(2,1)}), bf16[64,16,2048]{2,1,0:T(8,128)(2,1)}, u32[]{:S(2)}, u32[]{:S(2)}) async-start(bf16[64,16,2048]{2,1,0:T(8,128)(2,1)} %bitcast.570), calls=%async_computation.1 | async-start | bytes 8388608 | tf_op jit(solution)/shard_map/all_to_all | solution.py:232
  37.0 1.2 reduce_window_sum.27
  38.6 2.1 fusion
  40.9 2.5 convolution_convert_fusion.3
  46.1 2.2 all-gather.3
  49.9 15.3 %all-gather.4 = f32[4,258,128]{2,1,0:T(8,128)S(1)} all-gather(f32[1,258,128]{2,1,0:T(8,128)S(1)} %maximum_bitcast_fusion.1), channel_id=3, replica_groups=mesh['ep_0'=8,'ep_1'=4,'ep_2'=2,'tp'=4] {'ep_1'}, dimensions={0}, use_global_device_ids=true | all-gather | bytes 660480 | tf_op jit(solution)/shard_map/all_gather | solution.py:31
  67.3 74.5 %all-to-all-done.1 = bf16[64,16,2048]{2,1,0:T(8,128)(2,1)} async-done(((bf16[64,16,2048]{2,1,0:T(8,128)(2,1)}), bf16[64,16,2048]{2,1,0:T(8,128)(2,1)}, u32[]{:S(2)}, u32[]{:S(2)}) %all-to-all-start.1) | async-done | bytes 4194336 | tf_op jit(solution)/shard_map/all_to_all | solution.py:232
  141.8 4.7 %fusion.14 = f32[64,16,256]{2,1,0:T(8,128)} fusion(bf16[64,16,2048]{2,1,0:T(8,128)(2,1)} %all-to-all-done.1, bf16[1,2048,256]{2,1,0:T(8,128)(2,1)} %param.31), kind=kOutput, calls=%fused_computation.31 | convolution fusion | flops 1073741824 | bytes 6291456 | tf_op jit(solution)/shard_map/scd,df->scf/dot_general | solution.py:233
  146.5 9.1 %convolution_convert_fusion = bf16[64,16,2048]{2,1,0:T(8,128)(2,1)} fusion(bf16[64,16,2048]{2,1,0:T(8,128)(2,1)} %all-to-all-done.1, bf16[1,256,2048]{2,1,0:T(8,128)(2,1)S(1)} %copy-done, bf16[1,2048,256]{2,1,0:T(8,128)(2,1)} %param.32, f32[64,16,256]{2,1,0:T(8,128)} %fusion.14), kind=kOutput, calls=%fused_computation.10 | convolution fusion | flops 2151153664 | bytes 11534336 | tf_op jit(solution)/shard_map/scf,fo->sco/dot_general | solution.py:236
  155.7 3.3 %convolution_convert_fusion.4 = bf16[512,256]{1,0:T(8,128)(2,1)} fusion(bf16[2048,256]{1,0:T(8,128)(2,1)} %param.19, bf16[512,2048]{1,0:T(8,128)(2,1)} %param.17, f32[2048]{0:T(1024)S(1)} %copy-done.49, f32[512]{0:T(512)S(1)} %add_rsqrt_fusion), kind=kOutput, calls=%fused_computation.28 | convolution fusion | flops 541196288 | bytes 3418112 | tf_op jit(solution)/shard_map/dot_general | solution.py:153
  159.0 1.7 reshape.2597
  160.7 1.4 dynamic_slice.3
  169.0 1.3 add_maximum_fusion
  170.4 1.4 fusion.147
  171.7 1.8 multiply_add_fusion
  173.6 1.5 fusion.9
  175.0 2.5 multiply_reduce_fusion.1
  177.7 1.3 copy.118
  179.7 2.0 convolution_convert_fusion.1
  181.7 41.8 %all_to_all.15 = bf16[4,128,2048]{2,1,0:T(8,128)(2,1)} all-to-all(bf16[4,128,2048]{2,1,0:T(8,128)(2,1)S(1)} %bitcast.571), channel_id=1, replica_groups=mesh['ep_0'=8,'ep_1'=4,'ep_2'=2,'tp'=4] {'tp'}, dimensions={0} | all-to-all | bytes 4194304 | tf_op jit(solution)/shard_map/all_to_all | solution.py:63
  223.5 11.6 %all-to-all-start.2 = ((bf16[64,16,512]{2,1,0:T(8,128)(2,1)}), bf16[64,16,512]{2,1,0:T(8,128)(2,1)S(1)}, u32[]{:S(2)}, u32[]{:S(2)}) async-start(bf16[64,16,512]{2,1,0:T(8,128)(2,1)} %reduce-scatter.2.cloned.1.call-done), calls=%async_computation.3 | async-start | bytes 2097152 | tf_op jit(solution)/shard_map/all_to_all | solution.py:242
  236.1 1.4 fusion.159
  237.5 4.5 %gather_fusion.3 = f32[512]{0:T(512)S(1)} fusion(f32[256,64]{0,1:T(8,128)S(1)} %fusion.159, s32[512]{0:T(512)S(1)} %reshape.2644), kind=kCustom, calls=%fused_computation.3 | custom fusion | bytes 8192 | tf_op jit(solution)/shard_map/jit(take_along_axis)/gather | solution.py:128
  242.8 4.6 %gather_fusion.2 = f32[512]{0:T(512)S(1)} fusion(f32[256,16]{0,1:T(8,128)S(1)} %fusion.158, s32[512]{0:T(512)S(1)} %reshape.2638), kind=kCustom, calls=%fused_computation.2 | custom fusion | bytes 8192 | tf_op jit(solution)/shard_map/jit(take_along_axis)/gather | solution.py:129
  247.8 2.9 %reduce_sum.59 = bf16[128,2048]{1,0:T(8,128)(2,1)} reduce(bf16[4,128,2048]{2,1,0:T(8,128)(2,1)} %all_to_all.15, bf16[]{:T(256)} %constant.143.clone.1), dimensions={0}, to_apply=%region_5.6 | reduce | flops 786432 | bytes 2621442 | tf_op jit(solution)/shard_map/reduce_sum | solution.py:64
  250.7 12.5 %all-to-all-done.2 = bf16[64,16,512]{2,1,0:T(8,128)(2,1)S(1)} async-done(((bf16[64,16,512]{2,1,0:T(8,128)(2,1)}), bf16[64,16,512]{2,1,0:T(8,128)(2,1)S(1)}, u32[]{:S(2)}, u32[]{:S(2)}) %all-to-all-start.2) | async-done | bytes 1048608 | tf_op jit(solution)/shard_map/all_to_all | solution.py:242
  263.2 2.0 gather_fusion.1
  265.4 2.9 %multiply_reduce_fusion = bf16[256,512]{1,0:T(8,128)(2,1)} fusion(bf16[256,2,512]{2,1,0:T(2,128)(2,1)S(1)} %gather.19, pred[256,2]{1,0:T(8,128)(4,1)S(1)} %copy.124, f32[256,2]{1,0:T(8,128)S(1)} %copy.130), kind=kLoop, calls=%fused_computation.33 | loop fusion | flops 917504 | bytes 788992 | tf_op jit(solution)/shard_map/reduce_sum | solution.py:247
  (209 shorter events, 20.3 us)
Async XLA Ops:
  8.0 138.6 %copy-start = (bf16[1,256,2048]{2,1,0:T(8,128)(2,1)S(1)}, bf16[1,256,2048]{2,1,0:T(8,128)(2,1)}, u32[]{:S(2)}) copy-start(bf16[1,256,2048]{2,1,0:T(8,128)(2,1)} %param.33) | copy-start | bytes 3145732
  13.3 2.5 copy-start.16
  13.4 2.5 copy-start.24
  23.5 13.5 %copy-start.33 = (f32[2,512]{1,0:T(2,128)S(1)}, f32[2,512]{1,0:T(2,128)}, u32[]{:S(2)}) copy-start(f32[2,512]{1,0:T(2,128)} %param.23) | copy-start | bytes 12292
  23.5 17.4 %copy-start.47 = (bf16[2048,256]{1,0:T(8,128)(2,1)S(1)}, bf16[2048,256]{1,0:T(8,128)(2,1)}, u32[]{:S(2)}) copy-start(bf16[2048,256]{1,0:T(8,128)(2,1)} %param.20) | copy-start | bytes 3145732
  23.5 17.4 %copy-start.49 = (f32[2048]{0:T(1024)S(1)}, f32[2048]{0:T(1024)}, u32[]{:S(2)}) copy-start(f32[2048]{0:T(1024)} %param.18) | copy-start | bytes 24580
  23.5 118.3 %all-to-all-start.1 = ((bf16[64,16,2048]{2,1,0:T(8,128)(2,1)}), bf16[64,16,2048]{2,1,0:T(8,128)(2,1)}, u32[]{:S(2)}, u32[]{:S(2)}) async-start(bf16[64,16,2048]{2,1,0:T(8,128)(2,1)} %bitcast.570), calls=%async_computation.1 | async-start | bytes 8388608 | tf_op jit(solution)/shard_map/all_to_all | solution.py:232
  37.0 127.7 %all-gather.8.cloned.1.call-start = ((), (), s32[]{:S(2)}) async-start(), calls=%async_computation.5 | async-start | bytes 1216512 | tf_op jit(solution)/shard_map/all_gather | solution.py:31
  38.3 123.8 %copy-start.6 = (f32[4,2,128]{2,1,0:T(2,128)}, f32[4,2,128]{2,1,0:T(2,128)S(1)}, u32[]{:S(2)}) copy-start(f32[4,2,128]{2,1,0:T(2,128)S(1)} %reduce_window_sum.27) | copy-start | bytes 12292
  38.5 5.9 %copy-start.20 = (f32[2]{0:T(128)}, f32[2]{0:T(128)S(1)}, u32[]{:S(2)}) copy-start(f32[2]{0:T(128)S(1)} %get-tuple-element.4) | copy-start | bytes 28
  38.5 5.9 %copy-start.22 = (f32[2]{0:T(128)}, f32[2]{0:T(128)S(1)}, u32[]{:S(2)}) copy-start(f32[2]{0:T(128)S(1)} %get-tuple-element.2) | copy-start | bytes 28
  38.5 5.9 %copy-start.23 = (f32[2]{0:T(128)}, f32[2]{0:T(128)S(1)}, u32[]{:S(2)}) copy-start(f32[2]{0:T(128)S(1)} %get-tuple-element.3) | copy-start | bytes 28
  40.9 2.5 copy-start.1
  40.9 2.5 copy-start.48
  44.4 1.7 copy-start.9
  44.6 5.2 %copy-start.2 = (bf16[4,128,2,128]{3,2,1,0:T(2,128)(2,1)}, bf16[4,128,2,128]{3,2,1,0:T(2,128)(2,1)S(1)}, u32[]{:S(2)}) copy-start(bf16[4,128,2,128]{3,2,1,0:T(2,128)(2,1)S(1)} %reshape.2598) | copy-start | bytes 786436
  48.3 1.5 copy-start.18
  48.3 1.5 copy-start.19
  48.3 1.5 copy-start.21
  67.1 156.4 %reduce-scatter.2.cloned.1.call-start = ((), (), s32[]{:S(2)}) async-start(), calls=%async_computation.4 | async-start | bytes 5242880 | tf_op jit(solution)/shard_map/reduce_scatter | solution.py:239
  162.1 1.7 copy-start.11
  163.8 11.2 %copy-start.3 = (bf16[4,128,2,128]{3,2,1,0:T(2,128)(2,1)S(1)}, bf16[4,128,2,128]{3,2,1,0:T(2,128)(2,1)}, u32[]{:S(2)}) copy-start(bf16[4,128,2,128]{3,2,1,0:T(2,128)(2,1)} %copy-done.2) | copy-start | bytes 786436
  164.6 10.4 %copy-start.5 = (bf16[4,128,2,128]{1,3,2,0:T(8,128)(2,1)S(1)}, bf16[4,128,2,128]{1,3,2,0:T(8,128)(2,1)}, u32[]{:S(2)}) copy-start(bf16[4,128,2,128]{1,3,2,0:T(8,128)(2,1)} %copy-done.4) | copy-start | bytes 786436
  164.6 10.4 %copy-start.7 = (f32[4,2,128]{2,1,0:T(2,128)S(1)}, f32[4,2,128]{2,1,0:T(2,128)}, u32[]{:S(2)}) copy-start(f32[4,2,128]{2,1,0:T(2,128)} %copy-done.6) | copy-start | bytes 12292
  164.6 8.9 %copy-start.8 = (bf16[4,128,2,128]{3,2,1,0:T(2,128)(2,1)S(1)}, bf16[4,128,2,128]{3,2,1,0:T(2,128)(2,1)}, u32[]{:S(2)}) copy-start(bf16[4,128,2,128]{3,2,1,0:T(2,128)(2,1)} %reshape.2597) | copy-start | bytes 786436
  170.3 4.7 %copy-start.32 = (f32[4,2,128]{2,1,0:T(2,128)S(1)}, f32[4,2,128]{2,1,0:T(2,128)}, u32[]{:S(2)}) copy-start(f32[4,2,128]{2,1,0:T(2,128)} %add_maximum_fusion) | copy-start | bytes 12292
  173.5 6.1 %copy-start.31 = (f32[256]{0:T(256)S(1)}, f32[256]{0:T(256)}, u32[]{:S(2)}) copy-start(f32[256]{0:T(256)} %dynamic_slice.3) | copy-start | bytes 3076
  181.6 53.4 %copy-start.17 = (s32[512]{0:T(512)S(1)}, s32[512]{0:T(512)}, u32[]{:S(2)}) copy-start(s32[512]{0:T(512)} %copy-done.16) | copy-start | bytes 6148
  181.7 53.6 %copy-start.12 = (s32[256,2]{0,1:T(2,128)S(1)}, s32[256,2]{0,1:T(2,128)}, u32[]{:S(2)}) copy-start(s32[256,2]{0,1:T(2,128)} %param.30) | copy-start | bytes 6148
  223.5 39.8 %all-to-all-start.2 = ((bf16[64,16,512]{2,1,0:T(8,128)(2,1)}), bf16[64,16,512]{2,1,0:T(8,128)(2,1)S(1)}, u32[]{:S(2)}, u32[]{:S(2)}) async-start(bf16[64,16,512]{2,1,0:T(8,128)(2,1)} %reduce-scatter.2.cloned.1.call-done), calls=%async_computation.3 | async-start | bytes 2097152 | tf_op jit(solution)/shard_map/all_to_all | solution.py:242
  237.5 4.9 %copy-start.10 = (bf16[2048,16]{0,1:T(8,128)(2,1)S(1)}, bf16[2048,16]{0,1:T(8,128)(2,1)}, u32[]{:S(2)}) copy-start(bf16[2048,16]{0,1:T(8,128)(2,1)} %param.28) | copy-start | bytes 196612
  242.8 5.0 %copy-start.25 = (s32[512,1]{0,1:T(1,128)S(1)}, s32[512,1]{0,1:T(1,128)}, u32[]{:S(2)}) copy-start(s32[512,1]{0,1:T(1,128)} %copy-done.24) | copy-start | bytes 6148
  (22 other events, 15.8 us)
Sparse Core Ops, SparseCore 0:
  67.2 55.2 all-gather.7
Sparse Core Ops, SparseCore 1:
  155.8 66.6 reduce-scatter.1
where the time goes:
time: 277 us; the launch traced here: 276 us
  waiting for transfers between devices  87.1 us (31%)
  blocking collectives  59.3 us (21%)
  local copies, waits for them, and re-layouts  34.3 us (12%)
  matrix products  28.8 us (10%)
  starting transfers between devices  25.3 us (9%)
  other arithmetic  24.5 us (9%)
  between operations  16.5 us (6%)
    all_to_all x1, waiting for transfers between devices, shards(): lax.all_to_all(outgoing, EP, split_axis=0, concat_axis=0, tiled=True)  74.5 us
    all_to_all x1, blocking collectives, sum_at_owner(): parts = lax.all_to_all(split_up(x, dim, length), axis, 0, 0, tiled=True)  41.8 us
    all_gather x2, blocking collectives, collected_together(): both, at, found = (lax.all_gather(jnp.concatenate(lines), axis), 0, {})  17.5 us
    all_to_all x1, starting transfers between devices, shards(): lax.all_to_all(outgoing, EP, split_axis=0, concat_axis=0, tiled=True)  13.5 us
    all_to_all x1, waiting for transfers between devices, shards(): lax.all_to_all(summed, EP, split_axis=0, concat_axis=0, tiled=True)  12.5 us
    all_to_all x1, starting transfers between devices, shards(): lax.all_to_all(summed, EP, split_axis=0, concat_axis=0, tiled=True)  11.6 us
    dot_general x1, matrix products, shards(): jnp.einsum('scf,fo->sco', hidden, down_weight, preferred_element_type=jnp...  9.1 us
    gather x1, local copies, waits for them, and re-layouts, shards(): padded[owner // 2].reshape(expert_total, capacity, normed_b.shape[1])  5.98 us
  transfers between devices with their start and end apart: 4, of which 2 were waited for; matrix products, arithmetic and copies ran while one was open for 24% of the time, Pallas kernels for 0%

commit v1 on v0

--- a/solution.py
+++ b/solution.py
@@ -198,13 +198,13 @@
         head_gain, lax.axis_index("tp") * width_local, width_local
     ).reshape(head_local, head_size)
     cell_rows = rms_rows(cells, gain_local).reshape(row_count, width_local).astype(jnp.bfloat16)
-    mixer_out = sum_at_owner(
-        jnp.dot(cell_rows, mixer_out_weight, preferred_element_type=jnp.float32).astype(
-            jnp.bfloat16
-        ),
-        "tp",
-        0,
+    tp_count = lax.axis_size("tp")
+    out_weights = lax.all_gather(mixer_out_weight, "tp")
+    cell_groups = lax.all_to_all(split_up(cell_rows, 0, tp_count), "tp", 0, 0, tiled=True)
+    mixer_parts = jnp.einsum(
+        "gtw,gwo->gto", cell_groups, out_weights, preferred_element_type=jnp.float32
     ).astype(jnp.bfloat16)
+    mixer_out = jnp.sum(mixer_parts.astype(jnp.float32), axis=0).astype(jnp.bfloat16)
     normed_b = rms_rows(expert_in, expert_gain).astype(jnp.bfloat16)
     group_logits = jnp.dot(normed_b, group_router, preferred_element_type=jnp.float32)
     expert_logits = jnp.dot(normed_b, expert_router, preferred_element_type=jnp.float32)
@@ -224,21 +224,27 @@
         .at[slot_index]
         .set(jnp.arange(pair_total, dtype=jnp.int32))
     )
-    padded = jnp.concatenate([normed_b, jnp.zeros((1, normed_b.shape[1]), jnp.bfloat16)], axis=0)
-    outgoing = padded[owner // 2].reshape(expert_total, capacity, normed_b.shape[1])
+    share = normed_b.shape[1] // tp_count
+    own_share = lax.dynamic_slice_in_dim(normed_b, lax.axis_index("tp") * share, share, axis=1)
+    padded = jnp.concatenate([own_share, jnp.zeros((1, share), jnp.bfloat16)], axis=0)
+    outgoing = padded[owner // 2].reshape(expert_total, capacity, share)
     gate_weight = gate_experts[0]
     up_weight = up_experts[0]
     down_weight = down_experts[0]
+    down_parts = lax.all_to_all(split_up(down_weight, 1, tp_count), "tp", 0, 0, tiled=True)
     arrived = lax.all_to_all(outgoing, EP, split_axis=0, concat_axis=0, tiled=True)
-    gate_act = jnp.einsum("scd,df->scf", arrived, gate_weight, preferred_element_type=jnp.float32)
-    up_act = jnp.einsum("scd,df->scf", arrived, up_weight, preferred_element_type=jnp.float32)
+    arrived = lax.all_gather(arrived.reshape(-1, share), "tp")
+    gate_split = gate_weight.reshape(tp_count, share, -1)
+    up_split = up_weight.reshape(tp_count, share, -1)
+    gate_act = jnp.einsum("qsd,qdf->sf", arrived, gate_split, preferred_element_type=jnp.float32)
+    up_act = jnp.einsum("qsd,qdf->sf", arrived, up_split, preferred_element_type=jnp.float32)
     hidden = (jax.nn.silu(gate_act) * up_act).astype(jnp.bfloat16)
+    hidden = lax.all_gather(hidden, "tp")
     partial_rows = jnp.einsum(
-        "scf,fo->sco", hidden, down_weight, preferred_element_type=jnp.float32
-    )
-    summed = lax.psum_scatter(
-        partial_rows.astype(jnp.bfloat16), "tp", scatter_dimension=2, tiled=True
-    )
+        "gsf,gfo->gso", hidden, down_parts, preferred_element_type=jnp.float32
+    ).astype(jnp.bfloat16)
+    summed = jnp.sum(partial_rows.astype(jnp.float32), axis=0).astype(jnp.bfloat16)
+    summed = summed.reshape(expert_total, capacity, share)
     returned = lax.all_to_all(summed, EP, split_axis=0, concat_axis=0, tiled=True)
     picked = jnp.take(returned.reshape(-1, returned.shape[2]), slot_index, axis=0).astype(
         jnp.float32

time: 277 us -> 258 us (0.931)
  blocking collectives: 59.3 us -> 14.1 us
  local copies, waits for them, and re-layouts: 34.3 us -> 49.8 us
  starting transfers between devices: 25.3 us -> 32.1 us
  waiting for transfers between devices: 87.1 us -> 91.3 us
  matrix products: 28.8 us -> 32.1 us
    all_gather x0 -> x3, waiting for transfers between devices: none -> 67.7 us  [the longest x1 28.7 us: shards(): arrived = lax.all_gather(arrived.reshape(-1, share), 'tp')]
    all_to_all x1, waiting for transfers between devices: 74.5 us -> 10.8 us  [shards(): lax.all_to_all(outgoing, EP, split_axis=0, concat_axis=0, tiled=True)]
    all_to_all x1 -> x0, blocking collectives: 41.8 us -> none  [sum_at_owner(): parts = lax.all_to_all(split_up(x, dim, length), axis, 0, 0, tiled=True)]
    all_to_all x1, waiting for transfers between devices: 12.5 us -> 0.01 us  [shards(): lax.all_to_all(summed, EP, split_axis=0, concat_axis=0, tiled=True)]
    all_gather x1, waiting for transfers between devices: 0.01 us -> 12.4 us  [collected_together(): both, at, found = (lax.all_gather(jnp.concatenate(lines), axis), 0, {})]
    all_to_all x0 -> x2, starting transfers between devices: none -> 7.91 us  [the longest x1 4.27 us: shards(): lax.all_to_all(split_up(down_weight, 1, tp_count), 'tp', 0, 0, tiled=True)]
    unnamed x101 -> x104, local copies, waits for them, and re-layouts: 1.37 us -> 4.77 us
    all_gather x2, blocking collectives: 17.5 us -> 14.1 us  [collected_together(): both, at, found = (lax.all_gather(jnp.concatenate(lines), axis), 0, {})]
  transfers between devices with their start and end apart: 4 -> 8, of which waited for: 2 -> 5; matrix products, arithmetic and copies ran while one was open for 24% -> 32% of each run, Pallas kernels for 0% -> 0%
where the time goes in v1:
time: 258 us; the launch traced here: 256 us
  waiting for transfers between devices  91.3 us (35%)
  local copies, waits for them, and re-layouts  49.8 us (19%)
  starting transfers between devices  32.1 us (12%)
  matrix products  32.1 us (12%)
  other arithmetic  22.2 us (9%)
  between operations  14.8 us (6%)
  blocking collectives  14.1 us (5%)
    all_gather x1, waiting for transfers between devices, shards(): arrived = lax.all_gather(arrived.reshape(-1, share), 'tp')  28.7 us
    all_gather x1, waiting for transfers between devices, shards(): hidden = lax.all_gather(hidden, 'tp')  21.3 us
    all_gather x1, waiting for transfers between devices, shards(): out_weights = lax.all_gather(mixer_out_weight, 'tp')  17.7 us
    all_gather x2, blocking collectives, collected_together(): both, at, found = (lax.all_gather(jnp.concatenate(lines), axis), 0, {})  14.1 us
    all_to_all x1, starting transfers between devices, shards(): lax.all_to_all(outgoing, EP, split_axis=0, concat_axis=0, tiled=True)  13.3 us
    all_gather x1, waiting for transfers between devices, collected_together(): both, at, found = (lax.all_gather(jnp.concatenate(lines), axis), 0, {})  12.4 us
    all_to_all x1, waiting for transfers between devices, shards(): lax.all_to_all(outgoing, EP, split_axis=0, concat_axis=0, tiled=True)  10.8 us
    all_to_all x1, starting transfers between devices, shards(): lax.all_to_all(summed, EP, split_axis=0, concat_axis=0, tiled=True)  10.6 us
  transfers between devices with their start and end apart: 8, of which 5 were waited for; matrix products, arithmetic and copies ran while one was open for 32% of the time, Pallas kernels for 0%

profile of v1, /device:TPU:1, one launch (start us, length us, event | category | flops | bytes accessed | tf_op | source)
XLA Modules:
  0.0 256.4 jit_solution(11220169609391176731)
XLA Ops:
  12.6 2.4 scatter_custom_fusion
  16.7 5.1 %gather_fusion = bf16[1024,512]{1,0:T(8,128)(2,1)} fusion(bf16[257,512]{1,0:T(8,128)(2,1)S(1)} %concatenate.15, s32[1024]{0:T(1024)S(1)} %fusion.71), kind=kCustom, calls=%fused_computation | custom fusion | bytes 2101248 | tf_op jit(solution)/shard_map/gather | solution.py:230
  21.7 13.3 %all-to-all-start.1 = ((bf16[64,16,512]{2,1,0:T(8,128)(2,1)}), bf16[64,16,512]{2,1,0:T(8,128)(2,1)S(1)}, u32[]{:S(2)}, u32[]{:S(2)}) async-start(bf16[64,16,512]{2,1,0:T(8,128)(2,1)} %bitcast.108), calls=%async_computation.1 | async-start | bytes 2097152 | tf_op jit(solution)/shard_map/all_to_all | solution.py:235
  36.6 2.1 fusion
  38.7 3.3 %convolution_convert_fusion.1 = bf16[512,256]{1,0:T(8,128)(2,1)} fusion(bf16[2048,256]{1,0:T(8,128)(2,1)} %param.21, bf16[512,2048]{1,0:T(8,128)(2,1)} %param.17, f32[2048]{0:T(1024)S(1)} %copy-done.50, f32[512]{0:T(512)S(1)} %add_rsqrt_fusion), kind=kOutput, calls=%fused_computation.29 | convolution fusion | flops 541196288 | bytes 3418112 | tf_op jit(solution)/shard_map/dot_general | solution.py:157
  43.9 3.4 %convolution_convert_fusion.2 = bf16[512,256]{1,0:T(8,128)(2,1)} fusion(bf16[2048,256]{1,0:T(8,128)(2,1)} %param.20, bf16[512,2048]{1,0:T(8,128)(2,1)} %param.17, f32[2048]{0:T(1024)S(1)} %copy-done.50, f32[512]{0:T(512)S(1)} %add_rsqrt_fusion), kind=kOutput, calls=%fused_computation.30 | convolution fusion | flops 541196288 | bytes 3418112 | tf_op jit(solution)/shard_map/dot_general | solution.py:156
  47.3 1.7 reshape.2606
  50.0 2.4 fusion.22
  52.4 10.8 %all-to-all-done.1 = bf16[64,16,512]{2,1,0:T(8,128)(2,1)S(1)} async-done(((bf16[64,16,512]{2,1,0:T(8,128)(2,1)}), bf16[64,16,512]{2,1,0:T(8,128)(2,1)S(1)}, u32[]{:S(2)}, u32[]{:S(2)}) %all-to-all-start.1) | async-done | bytes 1048608 | tf_op jit(solution)/shard_map/all_to_all | solution.py:235
  65.8 2.8 %all-gather.5 = f32[2,258,128]{2,1,0:T(8,128)S(1)} all-gather(f32[1,258,128]{2,1,0:T(8,128)S(1)} %maximum_bitcast_fusion), channel_id=2, replica_groups=mesh['ep_0'=8,'ep_1'=4,'ep_2'=2,'tp'=4] {'ep_2'}, dimensions={0}, use_global_device_ids=true | all-gather | bytes 396288 | tf_op jit(solution)/shard_map/all_gather | solution.py:31
  69.8 11.4 %all-gather.6 = f32[4,258,128]{2,1,0:T(8,128)S(1)} all-gather(f32[1,258,128]{2,1,0:T(8,128)S(1)} %maximum_bitcast_fusion.1), channel_id=3, replica_groups=mesh['ep_0'=8,'ep_1'=4,'ep_2'=2,'tp'=4] {'ep_1'}, dimensions={0}, use_global_device_ids=true | all-gather | bytes 660480 | tf_op jit(solution)/shard_map/all_gather | solution.py:31
  83.2 28.7 %all-gather.13.cloned.1.call-done = bf16[4,1024,512]{2,1,0:T(8,128)(2,1)} async-done(((bf16[1,1024,512]{2,1,0:T(8,128)(2,1)}), bf16[4,1024,512]{2,1,0:T(8,128)(2,1)}) %all-gather.13.cloned.1.call-update) | async-done | bytes 4194320 | tf_op jit(solution)/shard_map/all_gather | solution.py:236
  111.9 3.6 %convolution_bitcast_fusion.1 = f32[1024,256]{1,0:T(8,128)S(1)} fusion(bf16[4,1024,512]{2,1,0:T(8,128)(2,1)} %all-gather.13.cloned.1.call-done, bf16[4,512,256]{2,1,0:T(8,128)(2,1)S(1)} %bitcast.563), kind=kOutput, calls=%fused_computation.20 | convolution fusion | flops 1073741824 | bytes 6291456 | tf_op jit(solution)/shard_map/qsd,qdf->sf/dot_general | solution.py:239
  115.6 2.1 fusion.8
  117.7 2.3 copy.133
  120.0 2.3 copy.134
  122.3 4.3 %all-to-all-start.2 = ((bf16[4,256,512]{2,1,0:T(8,128)(2,1)}), bf16[4,256,512]{2,1,0:T(8,128)(2,1)}, u32[]{:S(2)}, u32[]{:S(2)}) async-start(bf16[4,256,512]{2,1,0:T(8,128)(2,1)} %bitcast.566), calls=%async_computation.2 | async-start | bytes 2097152 | tf_op jit(solution)/shard_map/all_to_all | solution.py:234
  127.2 3.4 %convolution_convert_fusion.3 = bf16[512,256]{1,0:T(8,128)(2,1)} fusion(bf16[2048,256]{1,0:T(8,128)(2,1)} %param.19, bf16[512,2048]{1,0:T(8,128)(2,1)} %param.17, f32[2048]{0:T(1024)S(1)} %copy-done.50, f32[512]{0:T(512)S(1)} %add_rsqrt_fusion), kind=kOutput, calls=%fused_computation.31 | convolution fusion | flops 541196288 | bytes 3418112 | tf_op jit(solution)/shard_map/dot_general | solution.py:153
  131.6 1.7 reshape.2605
  136.1 12.4 %all-gather.19.cloned.1.call-done = f32[8,258,128]{2,1,0:T(8,128)} async-done(((f32[1,258,128]{2,1,0:T(8,128)}), f32[8,258,128]{2,1,0:T(8,128)}) %all-gather.19.cloned.1.call-update) | async-done | bytes 1056784 | tf_op jit(solution)/shard_map/all_gather | solution.py:31
  154.2 1.8 multiply_add_fusion
  158.2 2.5 multiply_reduce_fusion.1
  164.0 3.6 %all-to-all-start = ((bf16[4,128,256]{2,1,0:T(8,128)(2,1)}), bf16[4,128,256]{2,1,0:T(8,128)(2,1)S(1)}, u32[]{:S(2)}, u32[]{:S(2)}) async-start(bf16[4,128,256]{2,1,0:T(8,128)(2,1)} %multiply_convert_fusion), calls=%async_computation | async-start | bytes 524288 | tf_op jit(solution)/shard_map/all_to_all | solution.py:203
  167.7 21.3 %all-gather.17.cloned.1.call-done = bf16[4096,256]{1,0:T(8,128)(2,1)} async-done(((bf16[1024,256]{1,0:T(8,128)(2,1)}), bf16[4096,256]{1,0:T(8,128)(2,1)}) %all-gather.17.cloned.1.call-update) | async-done | bytes 2097168 | tf_op jit(solution)/shard_map/all_gather | solution.py:242
  189.0 4.3 %convert_reduce_fusion = bf16[1024,512]{1,0:T(8,128)(2,1)} fusion(bf16[4,1024,256]{2,1,0:T(8,128)(2,1)} %bitcast.611, bf16[4,256,512]{2,1,0:T(8,128)(2,1)} %all-to-all-done.2), kind=kOutput, calls=%fused_computation.10 | convolution fusion | flops 1077411840 | bytes 4194304 | tf_op jit(solution)/shard_map/gsf,gfo->gso/dot_general | solution.py:243
  193.3 10.6 %all-to-all-start.3 = ((bf16[64,16,512]{2,1,0:T(8,128)(2,1)}), bf16[64,16,512]{2,1,0:T(8,128)(2,1)S(1)}, u32[]{:S(2)}, u32[]{:S(2)}) async-start(bf16[64,16,512]{2,1,0:T(8,128)(2,1)} %bitcast.569), calls=%async_computation.3 | async-start | bytes 2097152 | tf_op jit(solution)/shard_map/all_to_all | solution.py:248
  208.5 4.5 %gather_fusion.3 = f32[512]{0:T(512)S(1)} fusion(f32[256,64]{0,1:T(8,128)S(1)} %fusion.145, s32[512]{0:T(512)S(1)} %reshape.2652), kind=kCustom, calls=%fused_computation.3 | custom fusion | bytes 8192 | tf_op jit(solution)/shard_map/jit(take_along_axis)/gather | solution.py:128
  217.2 4.5 %gather_fusion.2 = f32[512]{0:T(512)S(1)} fusion(f32[256,16]{0,1:T(8,128)S(1)} %fusion.144, s32[512]{0:T(512)S(1)} %reshape.2646), kind=kCustom, calls=%fused_computation.2 | custom fusion | bytes 8192 | tf_op jit(solution)/shard_map/jit(take_along_axis)/gather | solution.py:129
  223.2 17.7 %all-gather.15.cloned.1.call-done = bf16[1024,2048]{1,0:T(8,128)(2,1)} async-done(((bf16[256,2048]{1,0:T(8,128)(2,1)}), bf16[1024,2048]{1,0:T(8,128)(2,1)}) %all-gather.15.cloned.1.call-update) | async-done | bytes 4194320 | tf_op jit(solution)/shard_map/all_gather | solution.py:202
  240.9 3.8 %fusion.6 = bf16[128,2048]{1,0:T(8,128)(2,1)} fusion(bf16[4,128,256]{2,1,0:T(8,128)(2,1)S(1)} %all-to-all-done, bf16[4,256,2048]{2,1,0:T(8,128)(2,1)} %bitcast.565), kind=kOutput, calls=%fused_computation.17 | convolution fusion | flops 538705920 | bytes 4980736 | tf_op jit(solution)/shard_map/gtw,gwo->gto/dot_general | solution.py:204
  244.7 2.0 gather_fusion.1
  246.9 2.9 %multiply_reduce_fusion = bf16[256,512]{1,0:T(8,128)(2,1)} fusion(bf16[256,2,512]{2,1,0:T(2,128)(2,1)S(1)} %gather.19, pred[256,2]{1,0:T(8,128)(4,1)S(1)} %copy.131, f32[256,2]{1,0:T(8,128)S(1)} %copy-done.7), kind=kLoop, calls=%fused_computation.32 | loop fusion | flops 917504 | bytes 788992 | tf_op jit(solution)/shard_map/reduce_sum | solution.py:253
  (225 shorter events, 42.5 us)
Async XLA Ops:
  7.2 104.7 %copy-start = (bf16[1,2048,256]{2,1,0:T(8,128)(2,1)S(1)}, bf16[1,2048,256]{2,1,0:T(8,128)(2,1)}, u32[]{:S(2)}) copy-start(bf16[1,2048,256]{2,1,0:T(8,128)(2,1)} %param.31) | copy-start | bytes 3145732
  16.6 18.4 %copy-start.33 = (f32[2,512]{1,0:T(2,128)S(1)}, f32[2,512]{1,0:T(2,128)}, u32[]{:S(2)}) copy-start(f32[2,512]{1,0:T(2,128)} %param.23) | copy-start | bytes 12292
  21.7 17.0 %copy-start.50 = (f32[2048]{0:T(1024)S(1)}, f32[2048]{0:T(1024)}, u32[]{:S(2)}) copy-start(f32[2048]{0:T(1024)} %param.18) | copy-start | bytes 24580
  21.7 41.5 %all-to-all-start.1 = ((bf16[64,16,512]{2,1,0:T(8,128)(2,1)}), bf16[64,16,512]{2,1,0:T(8,128)(2,1)S(1)}, u32[]{:S(2)}, u32[]{:S(2)}) async-start(bf16[64,16,512]{2,1,0:T(8,128)(2,1)} %bitcast.108), calls=%async_computation.1 | async-start | bytes 2097152 | tf_op jit(solution)/shard_map/all_to_all | solution.py:235
  35.0 76.8 %all-gather.13.cloned.1.call-start = ((), (), s32[]{:S(2)}) async-start(), calls=%async_computation.4 | async-start | bytes 5242880 | tf_op jit(solution)/shard_map/all_gather | solution.py:236
  36.3 94.2 %copy-start.8 = (f32[4,2,128]{2,1,0:T(2,128)}, f32[4,2,128]{2,1,0:T(2,128)S(1)}, u32[]{:S(2)}) copy-start(f32[4,2,128]{2,1,0:T(2,128)S(1)} %reduce_window_sum.27) | copy-start | bytes 12292
  42.0 7.2 %copy-start.15 = (f32[2,512]{1,0:T(2,128)S(1)}, f32[2,512]{1,0:T(2,128)}, u32[]{:S(2)}) copy-start(f32[2,512]{1,0:T(2,128)} %param.22) | copy-start | bytes 12292
  49.3 16.4 %copy-start.23 = (f32[2]{0:T(128)}, f32[2]{0:T(128)S(1)}, u32[]{:S(2)}) copy-start(f32[2]{0:T(128)S(1)} %get-tuple-element.2) | copy-start | bytes 28
  49.3 16.4 %copy-start.24 = (f32[2]{0:T(128)}, f32[2]{0:T(128)S(1)}, u32[]{:S(2)}) copy-start(f32[2]{0:T(128)S(1)} %get-tuple-element.3) | copy-start | bytes 28
  49.5 16.3 %copy-start.10 = (f32[4,2]{1,0:T(4,128)}, f32[4,2]{1,0:T(4,128)S(1)}, u32[]{:S(2)}) copy-start(f32[4,2]{1,0:T(4,128)S(1)} %fusion.122) | copy-start | bytes 100
  64.2 84.3 %all-gather.19.cloned.1.call-start = ((), (), s32[]{:S(2)}) async-start(), calls=%async_computation.7 | async-start | bytes 1216512 | tf_op jit(solution)/shard_map/all_gather | solution.py:31
  68.6 13.3 %copy-start.19 = (f32[2,1,128]{2,1,0:T(1,128)}, f32[2,1,128]{2,1,0:T(1,128)S(1)}, u32[]{:S(2)}) copy-start(f32[2,1,128]{2,1,0:T(1,128)S(1)} %get-tuple-element.64) | copy-start | bytes 3076
  68.6 13.3 %copy-start.20 = (f32[2,1,128]{2,1,0:T(1,128)}, f32[2,1,128]{2,1,0:T(1,128)S(1)}, u32[]{:S(2)}) copy-start(f32[2,1,128]{2,1,0:T(1,128)S(1)} %get-tuple-element.65) | copy-start | bytes 3076
  68.6 13.3 %copy-start.22 = (f32[2]{0:T(128)}, f32[2]{0:T(128)S(1)}, u32[]{:S(2)}) copy-start(f32[2]{0:T(128)S(1)} %get-tuple-element.38) | copy-start | bytes 28
  68.6 13.3 %copy-start.28 = (f32[2]{0:T(128)}, f32[2]{0:T(128)S(1)}, u32[]{:S(2)}) copy-start(f32[2]{0:T(128)S(1)} %get-tuple-element.37) | copy-start | bytes 28
  68.6 13.2 %copy-start.35 = (f32[2]{0:T(128)}, f32[2]{0:T(128)S(1)}, u32[]{:S(2)}) copy-start(f32[2]{0:T(128)S(1)} %get-tuple-element.36) | copy-start | bytes 28
  69.2 12.6 %copy-start.46 = (f32[2]{0:T(128)}, f32[2]{0:T(128)S(1)}, u32[]{:S(2)}) copy-start(f32[2]{0:T(128)S(1)} %get-tuple-element.116) | copy-start | bytes 28
  69.2 12.6 %copy-start.44 = (f32[2]{0:T(128)}, f32[2]{0:T(128)S(1)}, u32[]{:S(2)}) copy-start(f32[2]{0:T(128)S(1)} %get-tuple-element.117) | copy-start | bytes 28
  69.2 12.6 %copy-start.45 = (f32[2]{0:T(128)}, f32[2]{0:T(128)S(1)}, u32[]{:S(2)}) copy-start(f32[2]{0:T(128)S(1)} %get-tuple-element.118) | copy-start | bytes 28
  83.1 105.9 %all-gather.17.cloned.1.call-start = ((), (), s32[]{:S(2)}) async-start(), calls=%async_computation.6 | async-start | bytes 2621440 | tf_op jit(solution)/shard_map/all_gather | solution.py:242
  122.3 41.7 %all-to-all-start.2 = ((bf16[4,256,512]{2,1,0:T(8,128)(2,1)}), bf16[4,256,512]{2,1,0:T(8,128)(2,1)}, u32[]{:S(2)}, u32[]{:S(2)}) async-start(bf16[4,256,512]{2,1,0:T(8,128)(2,1)} %bitcast.566), calls=%async_computation.2 | async-start | bytes 2097152 | tf_op jit(solution)/shard_map/all_to_all | solution.py:234
  126.6 114.3 %all-gather.15.cloned.1.call-start = ((), (), s32[]{:S(2)}) async-start(), calls=%async_computation.5 | async-start | bytes 5242880 | tf_op jit(solution)/shard_map/all_gather | solution.py:202
  127.2 27.0 %copy-start.2 = (f32[4,2,128,128]{3,2,1,0:T(8,128)S(1)}, f32[4,2,128,128]{3,2,1,0:T(8,128)}, u32[]{:S(2)}) copy-start(f32[4,2,128,128]{3,2,1,0:T(8,128)} %fusion.22) | copy-start | bytes 1572868
  135.4 22.9 %copy-start.4 = (bf16[4,128,2,128]{1,3,2,0:T(8,128)(2,1)S(1)}, bf16[4,128,2,128]{1,3,2,0:T(8,128)(2,1)}, u32[]{:S(2)}) copy-start(bf16[4,128,2,128]{1,3,2,0:T(8,128)(2,1)} %copy.118) | copy-start | bytes 786436
  136.1 22.1 %copy-start.5 = (bf16[4,128,2,128]{3,2,1,0:T(2,128)(2,1)S(1)}, bf16[4,128,2,128]{3,2,1,0:T(2,128)(2,1)}, u32[]{:S(2)}) copy-start(bf16[4,128,2,128]{3,2,1,0:T(2,128)(2,1)} %reshape.2606) | copy-start | bytes 786436
  148.6 7.5 %copy-start.9 = (bf16[4,128,2,128]{3,2,1,0:T(2,128)(2,1)S(1)}, bf16[4,128,2,128]{3,2,1,0:T(2,128)(2,1)}, u32[]{:S(2)}) copy-start(bf16[4,128,2,128]{3,2,1,0:T(2,128)(2,1)} %reshape.2605) | copy-start | bytes 786436
  156.0 7.2 %copy-start.34 = (f32[256]{0:T(256)S(1)}, f32[256]{0:T(256)}, u32[]{:S(2)}) copy-start(f32[256]{0:T(256)} %dynamic_slice.6) | copy-start | bytes 3076
  164.0 29.3 %all-to-all-start = ((bf16[4,128,256]{2,1,0:T(8,128)(2,1)}), bf16[4,128,256]{2,1,0:T(8,128)(2,1)S(1)}, u32[]{:S(2)}, u32[]{:S(2)}) async-start(bf16[4,128,256]{2,1,0:T(8,128)(2,1)} %multiply_convert_fusion), calls=%async_computation | async-start | bytes 524288 | tf_op jit(solution)/shard_map/all_to_all | solution.py:203
  189.0 14.9 %copy-start.18 = (s32[512]{0:T(512)S(1)}, s32[512]{0:T(512)}, u32[]{:S(2)}) copy-start(s32[512]{0:T(512)} %copy-done.17) | copy-start | bytes 6148
  189.0 15.7 %copy-start.13 = (s32[256,2]{0,1:T(2,128)S(1)}, s32[256,2]{0,1:T(2,128)}, u32[]{:S(2)}) copy-start(s32[256,2]{0,1:T(2,128)} %param.30) | copy-start | bytes 6148
  193.3 51.4 %all-to-all-start.3 = ((bf16[64,16,512]{2,1,0:T(8,128)(2,1)}), bf16[64,16,512]{2,1,0:T(8,128)(2,1)S(1)}, u32[]{:S(2)}, u32[]{:S(2)}) async-start(bf16[64,16,512]{2,1,0:T(8,128)(2,1)} %bitcast.569), calls=%async_computation.3 | async-start | bytes 2097152 | tf_op jit(solution)/shard_map/all_to_all | solution.py:248
  208.5 8.3 %copy-start.11 = (bf16[2048,16]{0,1:T(8,128)(2,1)S(1)}, bf16[2048,16]{0,1:T(8,128)(2,1)}, u32[]{:S(2)}) copy-start(bf16[2048,16]{0,1:T(8,128)(2,1)} %param.28) | copy-start | bytes 196612
  (27 other events, 53.2 us)
Sparse Core Ops, SparseCore 0:
  64.3 47.4 all-gather.12
  113.6 34.8 all-gather.18
  150.4 38.6 all-gather.16
  190.7 50.1 all-gather.14

commit v2 on v0

v2 whole, which is shorter than its diff:
```python
import functools
from types import SimpleNamespace

import jax
import jax.numpy as jnp
from jax import lax
from jax.experimental import pallas as pl
from jax.experimental.pallas import tpu as pltpu
from jax.sharding import PartitionSpec as P

MESH = pl.DeviceIdType.MESH
F32 = jnp.float32
BF16 = jnp.bfloat16
BLOCK = 128
CORES = 2
NEAR = 2
EPSILON = 1e-06
FLOOR = -1e30
HIGHEST = lax.Precision.HIGHEST
STATE_ROWS = BLOCK + 16


def dot(a, b, dims=((1,), (0,)), precision=None):
    return lax.dot_general(a, b, (dims, ((), ())), precision=precision, preferred_element_type=F32)


def split(x):
    high = x.astype(BF16)
    return high, (x - high.astype(F32)).astype(BF16)


def visits(nz):
    order = []
    for d in range(2, nz // 2 + 1):
        order += [d] if 2 * d == nz else [d, -d]
    return order + ([1] if nz == 2 else [-1, 1]) + [0]


def merge(earlier, later):
    peak = jnp.maximum(later[2] + earlier[1], later[1])
    fade_earlier = jnp.exp(later[2] + earlier[1] - peak)
    fade_later = jnp.exp(later[1] - peak)
    return (fade_earlier * earlier[0] + fade_later * later[0], peak, earlier[2] + later[2])


def identity(depth=BLOCK):
    return (
        jnp.zeros((depth, BLOCK), F32),
        jnp.full((1, BLOCK), FLOOR, F32),
        jnp.zeros((1, BLOCK), F32),
    )


def load_state(ref, n):
    depth = ref.shape[1] - 16
    return ref[n, 0:depth, :], ref[n, depth : depth + 1, :], ref[n, depth + 8 : depth + 9, :]


def store_state(ref, n, state):
    depth = ref.shape[1] - 16
    ref[n, 0:depth, :] = state[0]
    ref[n, depth : depth + 8, :] = jnp.broadcast_to(state[1], (8, BLOCK))
    ref[n, depth + 8 : depth + 16, :] = jnp.broadcast_to(state[2], (8, BLOCK))


def chosen(pred, a, b):
    return tuple(jnp.where(pred, s, t) for s, t in zip(a, b))


def log_sigmoid(x):
    small = jnp.exp(-jnp.abs(x))
    whole = 1.0 + small
    direct = jnp.log(whole) + (small - (whole - 1.0)) / whole
    series = small * (
        1.0 - small * (0.5 - small * (1.0 / 3.0 - small * (0.25 - small * (0.2 - small / 6.0))))
    )
    return jnp.minimum(x, 0.0) - jnp.where(small < 1.0 / 64.0, series, direct)


def norm_rows(src, dst, gain, rows, step, base=0):
    def body(i, carry):
        at = pl.ds(pl.multiple_of(base + i * step, step), step)
        wide = src[at, :].astype(F32)
        scaled = wide * lax.rsqrt(jnp.mean(wide * wide, axis=-1, keepdims=True) + EPSILON)
        dst[at, :] = (scaled * gain[...]).astype(BF16)
        return carry

    lax.fori_loop(0, rows // step, body, 0)


def kernel(dims, *refs):
    nz, ny, nx = dims.nz, dims.ny, dims.nx
    r = SimpleNamespace(**dict(zip(dims.names, refs)))
    plane = ny * CORES
    n_ep = nz * plane
    tokens = r.x_b.shape[0]
    width = r.x_b.shape[1]
    share = width // nx
    slots = r.outg.shape[0]
    cap = slots // n_ep
    chunk = plane * cap
    half = chunk // 2
    hid_w = r.gate.shape[1]
    heads = r.i_gate.shape[0]
    rows_a = r.x_a.shape[0]
    blocks = rows_a // BLOCK
    scale = BLOCK ** (-0.5)

    ep = lax.axis_index("ep")
    x = lax.axis_index("tp")
    z = lax.div(ep, plane)
    y = lax.div(lax.rem(ep, plane), CORES)
    c = lax.rem(ep, CORES)
    order = visits(nz)
    wide_from = nz - dims.near

    def offset(j):
        total = 0
        for k, d in enumerate(order):
            total = jnp.where(j == k, d, total)
        return total

    right = lax.rem(x + 1, nx)
    left = lax.rem(x + nx - 1, nx)
    mate = ep + 1 - 2 * c

    def rows(at, count, unit):
        return pl.ds(pl.multiple_of(at, unit), count)

    def remote(src, dst, send, recv, to_ep, to_x):
        return pltpu.make_async_remote_copy(
            src_ref=src,
            dst_ref=dst,
            send_sem=send,
            recv_sem=recv,
            device_id=(to_ep, to_x),
            device_id_type=MESH,
        )

    def settle(view, sem):
        pltpu.make_async_copy(view, view, sem).wait()

    barrier = pltpu.get_barrier_semaphore()

    def greet(k, carry):
        to = lax.rem(ep + k, n_ep)
        pl.semaphore_signal(barrier, inc=1, device_id=(to, x), device_id_type=MESH)
        return carry

    lax.fori_loop(1, n_ep, greet, 0)
    for k in range(1, nx):
        to = lax.rem(x + k, nx)
        pl.semaphore_signal(barrier, inc=1, device_id=(ep, to), device_id_type=MESH)

    down_at = r.down_h.at[:, rows(x * share, share, 128)]
    loads = SimpleNamespace()
    for n, (name, pair) in enumerate(
        dict(
            x_b=(r.x_b, r.xb),
            x_a=(r.x_a, r.xa),
            wq=(r.wq_h, r.wq),
            wk=(r.wk_h, r.wk),
            wv=(r.wv_h, r.wv),
            gate=(r.gate_h, r.gate),
            up=(r.up_h, r.up),
            group=(r.group_h, r.group),
            expert=(r.expert_h, r.expert),
            down=(down_at, r.down.at[x]),
            wout=(r.wout_h, r.wout.at[x]),
        ).items()
    ):
        load = pltpu.make_async_copy(*pair, r.load_s.at[n])
        setattr(loads, name, load)
    loads.x_b.start()

    route_rows = r.routes[...]
    experts_iota = lax.broadcasted_iota(jnp.int32, (n_ep, tokens), 0)
    hit0 = experts_iota == route_rows[0:1, :]
    hit1 = experts_iota == route_rows[1:2, :]
    named = jnp.where(hit0, 1.0, 0.0) + jnp.where(hit1, 1.0, 0.0)
    before = jnp.where(
        lax.broadcasted_iota(jnp.int32, (tokens, tokens), 0)
        < lax.broadcasted_iota(jnp.int32, (tokens, tokens), 1),
        1.0,
        0.0,
    ).astype(BF16)
    counts = dot(named.astype(BF16), before)
    place0 = jnp.sum(jnp.where(hit0, counts, 0.0), axis=0, keepdims=True)
    place1 = jnp.sum(jnp.where(hit1, counts, 0.0), axis=0, keepdims=True)
    route0 = route_rows[0:1, :].astype(F32)
    route1 = route_rows[1:2, :].astype(F32)
    slot0 = route0 * cap + place0
    slot1 = route1 * cap + place1
    flip = r.flip
    flip[...] = jnp.zeros_like(flip)
    flip[0:1, :] = route0
    flip[1:2, :] = route1
    flip[2:3, :] = slot0
    flip[3:4, :] = slot1
    r.cols[...] = jnp.transpose(flip[...])

    loads.x_b.wait()
    for load in list(vars(loads).values())[1:]:
        load.start()
    norm_rows(r.xb, r.nb, r.gain_b, tokens, min(32, tokens))

    def packed(j, wide):
        z_to = lax.rem(z - offset(j) + nz, nz)
        base = z_to * chunk
        place = (lax.broadcasted_iota(jnp.int32, (chunk, tokens), 0) + base).astype(F32)
        taken = jnp.where(place == flip[2:3, :], 1.0, 0.0) + jnp.where(
            place == flip[3:4, :], 1.0, 0.0
        )
        taken = taken.astype(BF16)
        if wide:
            for q in range(nx):
                part = r.nb[:, q * share : (q + 1) * share]
                r.near[j - wide_from, q, :, :] = dot(taken, part).astype(BF16)
        else:
            own = r.nb[:, rows(x * share, share, 128)]
            r.outg[rows(base, chunk, chunk), :] = dot(taken, own).astype(BF16)

    def pack_near(j, carry):
        packed(j, True)
        return carry

    def pack_far(j, carry):
        packed(j, False)
        return carry

    lax.fori_loop(0, wide_from, pack_far, 0)
    lax.fori_loop(wide_from, nz, pack_near, 0)

    pl.semaphore_wait(barrier, n_ep - 1 + nx - 1)

    far = lax.rem(x + 2, nx)
    fold = hid_w // 2
    for k, to in enumerate((right, left)):
        remote(
            r.down_h.at[:, rows(to * share, share, 128)],
            r.down.at[x],
            r.down_ss.at[k],
            r.down_rs.at[x],
            ep,
            to,
        ).start()
    for k, to in enumerate((right, left)):
        remote(
            r.down_h.at[k * fold : (k + 1) * fold, rows(far * share, share, 128)],
            r.relay.at[k],
            r.down_ss.at[2 + k],
            r.relay_rs.at[k],
            ep,
            to,
        ).start()

    def pass_down():
        for k, (source_x, to) in enumerate(((left, right), (right, left))):
            settle(r.relay.at[k], r.relay_rs.at[k])
            remote(
                r.relay.at[k],
                r.down.at[source_x, k * fold : (k + 1) * fold, :],
                r.down_ss.at[4 + k],
                r.far_rs.at[k],
                ep,
                to,
            ).start()

    def posted(j, wide):
        z_to = lax.rem(z - offset(j) + nz, nz)

        def post(k, inner):
            to = z_to * plane + k

            @pl.when(to != ep)
            def _():
                if wide:
                    src = r.near.at[j - wide_from, :, rows(k * cap, cap, cap), :]
                    dst = r.tok.at[:, rows(ep * cap, cap, cap), :]
                else:
                    src = r.outg.at[rows(to * cap, cap, cap), :]
                    dst = r.tok.at[x, rows(ep * cap, cap, cap), :]
                remote(src, dst, r.disp_ss.at[z_to], r.disp_rs.at[z], to, x).start()

            return inner

        lax.fori_loop(0, plane, post, 0)

    def post_near(j, carry):
        posted(j, True)
        return carry

    def post_far(j, carry):
        posted(j, False)
        return carry

    lax.fori_loop(0, wide_from, post_far, 0)
    lax.fori_loop(wide_from, nz, post_near, 0)
    own_rows = rows(ep * cap, cap, cap)
    own_place = rows(lax.rem(ep, plane) * cap, cap, cap)
    kept = pltpu.make_async_copy(
        r.near.at[dims.near - 1, :, own_place, :], r.tok.at[:, own_rows, :], r.kept_s.at[0]
    )
    kept.start()

    def ring_of(me, count, device):
        after, ahead = lax.rem(me + 1, count), lax.rem(me + count - 1, count)
        return SimpleNamespace(
            me=me,
            right=after,
            left=ahead,
            far=lax.rem(me + 2, count),
            to_right=device(after),
            to_left=device(ahead),
        )

    over_x = ring_of(x, nx, lambda to: (ep, to))
    over_y = ring_of(y, ny, lambda to: (z * plane + to * CORES + c, x))

    def ring_start(ring, view, src, ss, rs, j):
        remote(src, view(ring.me), ss.at[0, j], rs.at[0, j], *ring.to_right).start()
        remote(src, view(ring.me), ss.at[1, j], rs.at[1, j], *ring.to_left).start()

    def ring_forward(ring, view, low, high, ss, rs, j):
        settle(view(ring.left), rs.at[0, j])
        part = low(ring.left)
        remote(part, part, ss.at[2, j], rs.at[2, j], *ring.to_right).start()
        settle(view(ring.right), rs.at[1, j])
        part = high(ring.right)
        remote(part, part, ss.at[3, j], rs.at[3, j], *ring.to_left).start()

    def ring_finish(ring, low, high, rs, j):
        settle(low(ring.far), rs.at[2, j])
        settle(high(ring.far), rs.at[3, j])

    def ring_sent(ring, view, low, high, ss, j):
        settle(view(ring.me), ss.at[0, j])
        settle(view(ring.me), ss.at[1, j])
        settle(low(ring.left), ss.at[2, j])
        settle(high(ring.right), ss.at[3, j])

    def source(j):
        return lax.rem(z + offset(j) + nz, nz)

    def tok_views(j):
        base = source(j) * chunk
        return (
            lambda q: r.tok.at[q, rows(base, chunk, chunk), :],
            lambda q: r.tok.at[q, rows(base, half, half), :],
            lambda q: r.tok.at[q, rows(base + half, half, half), :],
        )

    def hid_views(j):
        base = source(j) * chunk
        return (
            lambda q: r.hid.at[q, rows(base, chunk, chunk), :],
            lambda q: r.hid.at[q, rows(base, half, half), :],
            lambda q: r.hid.at[q, rows(base + half, half, half), :],
        )

    out_half = r.wout.shape[1] // CORES
    out_part = out_half // ny

    def wout_views(q=None):
        def cut(base, count):
            def view(n):
                at, place = (n, y) if q is None else (q, n)
                return r.wout.at[at, rows(c * out_half + place * out_part + base, count, 16), :]

            return view

        return cut(0, out_part), cut(0, out_part // 2), cut(out_part // 2, out_part // 2)

    others = [lax.rem(x + k, nx) for k in range(1, nx)]

    def wout_half(q):
        return r.wout.at[q, rows(c * out_half, out_half, out_half), :]

    def take_rows(j):
        view, low, high = tok_views(j)
        settle(view(x), r.disp_rs.at[source(j)])
        ring_start(over_x, view, view(x), r.tok_ss, r.tok_rs, j)

    def expand(j):
        view, low, high = tok_views(j)
        at = rows(source(j) * chunk, chunk, chunk)

        @pl.when(j == nz - 1)
        def _():
            settle(r.near.at[0, :, rows(0, chunk - cap, cap), :], r.disp_rs.at[z])
            kept.wait()

        @pl.when(jnp.logical_and(j >= wide_from, j < nz - 1))
        def _():
            settle(r.tok.at[:, at, :], r.disp_rs.at[source(j)])

        @pl.when(j < wide_from)
        def _():
            ring_finish(over_x, low, high, r.tok_rs, j)

        gated = jnp.zeros((chunk, hid_w), F32)
        upped = jnp.zeros((chunk, hid_w), F32)
        for q in range(nx):
            part = r.tok[q, at, :]
            gated += dot(part, r.gate[q * share : (q + 1) * share, :])
            upped += dot(part, r.up[q * share : (q + 1) * share, :])
        r.hid[x, at, :] = (gated * jax.nn.sigmoid(gated) * upped).astype(BF16)
        hview = hid_views(j)[0]
        ring_start(over_x, hview, hview(x), r.hid_ss, r.hid_rs, j)

    def contract(j):
        view, low, high = hid_views(j)
        ring_finish(over_x, low, high, r.hid_rs, j)
        z_to = source(j)
        at = rows(z_to * chunk, chunk, chunk)
        total = jnp.zeros((chunk, share), F32)
        for q in range(nx):
            total += dot(r.hid[q, at, :], r.down[q]).astype(BF16).astype(F32)
        r.res[at, :] = total.astype(BF16)

        def post(k, inner):
            to = z_to * plane + k

            @pl.when(to != ep)
            def _():
                remote(
                    r.res.at[rows(to * cap, cap, cap), :],
                    r.ret.at[rows(ep * cap, cap, cap), :],
                    r.ret_ss.at[z_to],
                    r.ret_rs.at[z],
                    to,
                    x,
                ).start()

            return inner

        lax.fori_loop(0, plane, post, 0)

        @pl.when(j == nz - 1)
        def _():
            pltpu.make_async_copy(
                r.res.at[own_rows, :], r.ret.at[own_rows, :], r.kept_s.at[1]
            ).start()

    def gather_up(j):
        z_from = lax.rem(z - offset(j) + nz, nz)
        base = z_from * chunk
        at = rows(base, chunk, chunk)

        @pl.when(j == 0)
        def _():
            r.acc[...] = jnp.zeros_like(r.acc)

        @pl.when(j == nz - 1)
        def _():
            settle(r.res.at[rows(0, chunk - cap, cap), :], r.ret_rs.at[z])
            settle(r.res.at[rows(0, cap, cap), :], r.kept_s.at[1])

        @pl.when(j < nz - 1)
        def _():
            settle(r.ret.at[at, :], r.ret_rs.at[z_from])

        lane = (lax.broadcasted_iota(jnp.int32, (tokens, chunk), 1) + base).astype(F32)
        back = r.ret[at, :]
        for k in range(2):
            picks = jnp.where(lane == r.cols[:, 2 + k : 3 + k], 1.0, 0.0).astype(BF16)
            r.acc[...] += r.comb[:, k : k + 1] * dot(picks, back)

    def weights():
        loads.group.wait()
        loads.expert.wait()
        normed = r.nb[...]
        group_logits = dot(normed, r.group[...], ((1,), (1,)))
        expert_logits = dot(normed, r.expert[...], ((1,), (1,)))
        members = expert_logits.shape[1] // group_logits.shape[1]
        groups_iota = lax.broadcasted_iota(jnp.int32, group_logits.shape, 1)
        lanes_iota = lax.broadcasted_iota(jnp.int32, expert_logits.shape, 1)
        picked, grouped = [], []
        for k in range(2):
            route = r.cols[:, k : k + 1].astype(jnp.int32)
            picked.append(
                jnp.sum(jnp.where(lanes_iota == route, expert_logits, 0.0), axis=1, keepdims=True)
            )
            first = route - groups_iota * members
            inside = jnp.logical_and(first >= 0, first < members)
            grouped.append(jnp.sum(jnp.where(inside, group_logits, 0.0), axis=1, keepdims=True))
        for k in range(2):
            r.comb[:, k : k + 1] = jax.nn.sigmoid(grouped[k]) * jax.nn.sigmoid(
                picked[k] - picked[1 - k]
            )

    def project(first, last):
        if first == 0:
            loads.x_a.wait()
            loads.wq.wait()
            loads.wk.wait()
            loads.wv.wait()

        def body(b, carry):
            at = rows(b * BLOCK, BLOCK, BLOCK)
            norm_rows(r.xa, r.na, r.gain_a, BLOCK, 32, b * BLOCK)
            normed = r.na[at, :]
            for weight, to in ((r.wq, r.q), (r.wk, r.k), (r.wv, r.v)):
                to[at, :] = dot(normed, weight[...]).astype(BF16)
            return carry

        lax.fori_loop(first, last, body, 0)

    def pieces(n):
        h, b = n // blocks, n % blocks
        at = (slice(b * BLOCK, (b + 1) * BLOCK), slice(h * BLOCK, (h + 1) * BLOCK))
        return r.q[at], r.k[at], r.v[at]

    def summarize():
        logs = log_sigmoid(r.f_gate[...])
        inputs = r.i_gate[...]
        gates = r.gates
        for n in range(heads * blocks):
            h, b = n // blocks, n % blocks
            lanes = slice(b * BLOCK, (b + 1) * BLOCK)
            gates[n : n + 1, :] = logs[h : h + 1, lanes]
            gates[16 + n : 17 + n, :] = inputs[h : h + 1, lanes]
        upto = jnp.where(
            lax.broadcasted_iota(jnp.int32, (BLOCK, BLOCK), 0)
            <= lax.broadcasted_iota(jnp.int32, (BLOCK, BLOCK), 1),
            1.0,
            0.0,
        )
        count = heads * blocks
        sums = dot(gates[0:count, :], upto, precision=HIGHEST)
        totals = sums[:, BLOCK - 1 : BLOCK]
        log_weight = totals - sums + gates[16 : 16 + count, :]
        peaks = jnp.max(log_weight, axis=1, keepdims=True)
        turn = r.turn
        turn[...] = jnp.zeros_like(turn)
        turn[0:count, :] = sums
        turn[count : 2 * count, :] = jnp.exp(log_weight - peaks)
        turned = jnp.transpose(turn[...])
        r.turned[...] = turned
        for h in range(heads):
            summary = None
            for b in range(blocks):
                n = h * blocks + b
                _, keys, values = pieces(n)
                high, low = split(values.astype(F32) * turned[:, count + n : count + n + 1])
                memory = scale * (dot(keys, high, ((0,), (0,))) + dot(keys, low, ((0,), (0,))))
                state = (
                    memory,
                    jnp.broadcast_to(peaks[n : n + 1, :], (1, BLOCK)),
                    jnp.broadcast_to(totals[n : n + 1, :], (1, BLOCK)),
                )
                store_state(r.sums, n, state)
                summary = state if summary is None else merge(summary, state)
            store_state(r.own, h, summary)
        remote(r.own, r.other, r.mate_ss.at[0], r.mate_rs.at[0], mate, x).start()

    def chip_level():
        settle(r.other, r.mate_rs.at[0])
        mine, theirs = load_state(r.own, c), load_state(r.other, c)
        first = c == 0
        store_state(
            r.y_in, y, merge(chosen(first, mine, theirs), chosen(first, theirs, mine))
        )
        for k in range(1, ny):
            y_to = lax.rem(y + k, ny)
            remote(
                r.y_in.at[y],
                r.y_in.at[y],
                r.y_ss.at[k],
                r.y_rs.at[y],
                z * plane + y_to * CORES + c,
                x,
            ).start()

    def run_up(ref, count, place, run):
        depth = run.shape[1] - 16
        store_state(run, 0, identity(depth))
        store_state(run, 1, identity(depth))

        def body(k, carry):
            after = merge(load_state(run, 1), load_state(ref, k))

            store_state(run, 1, after)

            @pl.when(k + 1 == place)
            def _():
                store_state(run, 0, after)

            return carry

        lax.fori_loop(0, count, body, 0)

    def plane_level():
        for k in range(1, ny):
            y_from = lax.rem(y + k, ny)
            settle(r.y_in.at[y_from], r.y_rs.at[y_from])
        run_up(r.y_in, ny, y, r.y_run)
        _, peak, total = load_state(r.y_run, 1)
        part = r.z_in.shape[1] - 16
        store_state(r.z_in, z, (r.y_run[1, rows(y * part, part, part), :], peak, total))
        for k in range(1, nz):
            z_to = lax.rem(z + k, nz)
            remote(
                r.z_in.at[z],
                r.z_in.at[z],
                r.z_ss.at[k],
                r.z_rs.at[z],
                z_to * plane + y * CORES + c,
                x,
            ).start()

    def line_level():
        for k in range(1, nz):
            z_from = lax.rem(z + k, nz)
            settle(r.z_in.at[z_from], r.z_rs.at[z_from])
        run_up(r.z_in, nz, z, r.z_run)
        store_state(r.line, y, load_state(r.z_run, 0))
        for k in range(1, ny):
            y_to = lax.rem(y + k, ny)
            remote(
                r.line.at[y],
                r.line.at[y],
                r.line_ss.at[k],
                r.line_rs.at[y],
                z * plane + y_to * CORES + c,
                x,
            ).start()

    def start_level():
        for k in range(1, ny):
            y_from = lax.rem(y + k, ny)
            settle(r.line.at[y_from], r.line_rs.at[y_from])
        parts = [load_state(r.line, k) for k in range(ny)]
        memory = jnp.concatenate([part[0] for part in parts], axis=0)
        store_state(r.start, c, merge((memory, *parts[0][1:]), load_state(r.y_run, 0)))
        remote(
            r.start.at[c],
            r.start.at[c],
            r.mate_ss.at[1],
            r.mate_rs.at[1],
            mate,
            x,
        ).start()

    def attend(first, last):
        if first == 0:
            settle(r.start.at[1 - c], r.mate_rs.at[1])
        count = heads * blocks
        turned = r.turned
        gates = r.gates
        states = []
        for h in range(heads):
            if first == 0:
                later = chosen(c == 1, load_state(r.other, h), identity())
                states.append(merge(load_state(r.start, h), later))
            else:
                states.append(load_state(r.current, h))
        causal = lax.broadcasted_iota(jnp.int32, (BLOCK, BLOCK), 0) >= lax.broadcasted_iota(
            jnp.int32, (BLOCK, BLOCK), 1
        )
        for b in range(first, last):
            for h in range(heads):
                n = h * blocks + b
                queries, keys, values = pieces(n)
                memory, peak, _ = states[h]
                column = turned[:, n : n + 1]
                within = column - r.turn[n : n + 1, :] + gates[16 + n : 17 + n, :]
                within = jnp.where(causal, within, FLOOR)
                carried = column + peak[:, 0:1]
                top = jnp.maximum(jnp.max(within, axis=1, keepdims=True), carried)
                raw = dot(queries, keys, ((1,), (1,))) * scale
                scores = (raw * jnp.exp(within - top)).astype(BF16)
                high, low = split(memory)
                recalled = dot(queries, high) + dot(queries, low)
                cells = dot(scores, values) + jnp.exp(carried - top) * recalled
                square = jnp.mean(cells * cells, axis=1, keepdims=True)
                gain = r.gain_h[pl.ds(x * heads + h, 1), :]
                r.cell[b, :, h * BLOCK : (h + 1) * BLOCK] = (
                    cells * lax.rsqrt(square + EPSILON) * gain
                ).astype(BF16)
                if b + 1 < blocks:
                    states[h] = merge(states[h], load_state(r.sums, n))
        if last < blocks:
            for h in range(heads):
                store_state(r.current, h, states[h])
            return
        for k in range(1, nx):
            to = lax.rem(x + k, nx)
            remote(
                r.cell.at[to],
                r.cells.at[x],
                r.cell_ss.at[k],
                r.cell_rs.at[x],
                ep,
                to,
            ).start()
        r.cells[x] = r.cell[x]

    def mix_out():
        for k in range(1, nx):
            q = lax.rem(x + k, nx)
            settle(r.cells.at[q], r.cell_rs.at[q])
            other_half = rows((1 - c) * out_half, out_half, out_half)
            settle(r.wout.at[q, other_half, :], r.wm_rs.at[q])
        loads.wout.wait()
        step = r.mixed.shape[1] // 4
        for n in range(4):
            lanes = slice(n * step, (n + 1) * step)
            total = jnp.zeros((BLOCK, step), F32)
            for g in range(nx):
                total += dot(r.cells[g], r.wout[g, :, lanes]).astype(BF16).astype(F32)
            r.mixed[:, lanes] = total.astype(BF16)
        pltpu.make_async_copy(r.mixed, r.out_a, r.out_s.at[0]).start()

    when, lag = dims.when, dims.lag

    def at_step(number, job):
        @pl.when(jnp.logical_and(number >= 0, number < nz))
        def _():
            job(number)

    def far_only(job):
        def run(j):
            @pl.when(j < wide_from)
            def _():
                job(j)

        return run

    def forward_rows(j):
        ring_forward(over_x, *tok_views(j), r.tok_ss, r.tok_rs, j)

    def forward_hidden(j):
        ring_forward(over_x, *hid_views(j), r.hid_ss, r.hid_rs, j)

    def down_arrived():
        loads.down.wait()
        for k, source_x in enumerate((left, right)):
            settle(r.down.at[source_x], r.down_rs.at[source_x])
            settle(r.relay.at[k], r.far_rs.at[k])

    def experts_arrived():
        loads.gate.wait()
        loads.up.wait()

    def wout_start():
        own = r.wout_h.at[rows(c * out_half + y * out_part, out_part, 16), :]
        ring_start(over_x, wout_views()[0], own, r.w_ss, r.w_rs, 0)

    def wout_forward():
        ring_forward(over_x, *wout_views(), r.w_ss, r.w_rs, 0)

    def wout_turn():
        ring_finish(over_x, *wout_views()[1:], r.w_rs, 0)
        for k, q in enumerate(others):
            view = wout_views(q)[0]
            ring_start(over_y, view, view(y), r.wy_ss, r.wy_rs, k)

    def wout_pass():
        for k, q in enumerate(others):
            ring_forward(over_y, *wout_views(q), r.wy_ss, r.wy_rs, k)

    def wout_spread():
        for k, q in enumerate(others):
            ring_finish(over_y, *wout_views(q)[1:], r.wy_rs, k)
            half = wout_half(q)
            remote(half, half, r.wm_ss.at[k], r.wm_rs.at[q], mate, x).start()

    first_jobs = ((lag.expand, experts_arrived), (lag.contract, down_arrived))
    jobs = (
        (when.pass_down, pass_down),
        (when.wout_start, wout_start),
        (when.chip, chip_level),
        (when.plane, plane_level),
        (when.wout_forward, wout_forward),
        (when.line, line_level),
        (when.start, start_level),
        (when.weights, weights),
        (when.attend, functools.partial(attend, 0, blocks // 2)),
        (when.attend + 1, functools.partial(attend, blocks // 2, blocks)),
        (when.wout_turn, wout_turn),
        (when.wout_pass, wout_pass),
        (when.wout_spread, wout_spread),
        (when.mix, mix_out),
    )
    project(0, blocks)
    summarize()

    def step(i, carry):
        at_step(i - lag.take, far_only(take_rows))
        at_step(i - lag.forward, far_only(forward_rows))
        for place, job in first_jobs:
            pl.when(i == place)(job)
        at_step(i - lag.expand, expand)
        at_step(i - lag.hidden, forward_hidden)
        at_step(i - lag.contract, contract)
        at_step(i - lag.gather, gather_up)
        for place, job in jobs:
            pl.when(i == place)(job)
        return carry

    lax.fori_loop(0, max(nz + lag.gather, when.mix + 1), step, 0)

    r.mixed_b[...] = r.acc[...].astype(BF16)
    last = pltpu.make_async_copy(r.mixed_b, r.out_b, r.out_s.at[1])
    last.start()

    def sent(j, carry):
        z_to = lax.rem(z - offset(j) + nz, nz)
        ring_sent(over_x, *hid_views(j), r.hid_ss, j)

        @pl.when(j == nz - 1)
        def _():
            settle(r.near.at[0, :, rows(0, chunk - cap, cap), :], r.disp_ss.at[z])
            settle(r.res.at[rows(0, chunk - cap, cap), :], r.ret_ss.at[z])

        @pl.when(j < nz - 1)
        def _():
            settle(r.res.at[rows(0, chunk, chunk), :], r.ret_ss.at[z_to])

        @pl.when(jnp.logical_and(j >= wide_from, j < nz - 1))
        def _():
            settle(r.near.at[0], r.disp_ss.at[z_to])

        @pl.when(j < wide_from)
        def _():
            settle(r.outg.at[rows(0, chunk, chunk), :], r.disp_ss.at[z_to])
            ring_sent(over_x, *tok_views(j), r.tok_ss, j)

        return carry

    lax.fori_loop(0, nz, sent, 0)
    ring_sent(over_x, *wout_views(), r.w_ss, 0)
    for k, q in enumerate(others):
        ring_sent(over_y, *wout_views(q), r.wy_ss, k)
        settle(wout_half(q), r.wm_ss.at[k])
        settle(r.cell.at[x], r.cell_ss.at[k + 1])
    for k in range(2):
        settle(r.down.at[x], r.down_ss.at[k])
        settle(r.relay.at[0], r.down_ss.at[k + 2])
        settle(r.relay.at[0], r.down_ss.at[k + 4])
    for k in range(1, ny):
        settle(r.y_in.at[y], r.y_ss.at[k])
        settle(r.line.at[y], r.line_ss.at[k])
    for k in range(1, nz):
        settle(r.z_in.at[z], r.z_ss.at[k])
    settle(r.own, r.mate_ss.at[0])
    settle(r.start.at[c], r.mate_ss.at[1])
    settle(r.mixed, r.out_s.at[0])
    last.wait()


def solution(mesh, shape=(8, 4)):
    nz, ny = shape
    nx = mesh.shape["tp"]
    n_ep = mesh.shape["ep"]

    def shards(
        mixer_in,
        mixer_gain,
        query_weight,
        key_weight,
        value_weight,
        input_gate,
        forget_gate,
        head_gain,
        mixer_out_weight,
        expert_in,
        expert_gain,
        group_router,
        expert_router,
        routes,
        gate_experts,
        up_experts,
        down_experts,
    ):
        rows_a, width = mixer_in.shape
        near = min(NEAR, nz - 1)
        tokens = expert_in.shape[0]
        share = width // nx
        cap = 4 * tokens // n_ep
        slots = n_ep * cap
        heads = input_gate.shape[0]
        blocks = rows_a // BLOCK
        qkv = query_weight.shape[1]
        hid_w = gate_experts.shape[2]
        vmem = pl.BlockSpec(memory_space=pltpu.VMEM)
        hbm = pl.BlockSpec(memory_space=pl.ANY)
        inputs = dict(
            x_a=(mixer_in, hbm),
            gain_a=(mixer_gain.reshape(1, -1), vmem),
            wq_h=(query_weight, hbm),
            wk_h=(key_weight, hbm),
            wv_h=(value_weight, hbm),
            i_gate=(input_gate, vmem),
            f_gate=(forget_gate, vmem),
            gain_h=(head_gain.reshape(-1, BLOCK), vmem),
            wout_h=(mixer_out_weight, hbm),
            x_b=(expert_in, hbm),
            gain_b=(expert_gain.reshape(1, -1), vmem),
            group_h=(group_router.T, hbm),
            expert_h=(expert_router.T, hbm),
            routes=(routes.T, vmem),
            gate_h=(gate_experts[0], hbm),
            up_h=(up_experts[0], hbm),
            down_h=(down_experts[0], hbm),
        )
        state = (STATE_ROWS, BLOCK)
        part = (BLOCK // ny + 16, BLOCK)
        dma = pltpu.SemaphoreType.DMA
        scratch = dict(
            xa=pltpu.VMEM((rows_a, width), BF16),
            xb=pltpu.VMEM((tokens, width), BF16),
            wq=pltpu.VMEM(query_weight.shape, BF16),
            wk=pltpu.VMEM(query_weight.shape, BF16),
            wv=pltpu.VMEM(query_weight.shape, BF16),
            gate=pltpu.VMEM((width, hid_w), BF16),
            up=pltpu.VMEM((width, hid_w), BF16),
            group=pltpu.VMEM(group_router.shape[::-1], BF16),
            expert=pltpu.VMEM(expert_router.shape[::-1], BF16),
            down=pltpu.VMEM((nx, hid_w, share), BF16),
            relay=pltpu.VMEM((2, hid_w // 2, share), BF16),
            wout=pltpu.VMEM((nx, qkv, mixer_out_weight.shape[1]), BF16),
            flip=pltpu.VMEM((128, tokens), F32),
            cols=pltpu.VMEM((tokens, 128), F32),
            nb=pltpu.VMEM((tokens, width), BF16),
            outg=pltpu.VMEM((slots, share), BF16),
            near=pltpu.VMEM((near, nx, slots // nz, share), BF16),
            tok=pltpu.VMEM((nx, slots, share), BF16),
            hid=pltpu.VMEM((nx, slots, hid_w), BF16),
            res=pltpu.VMEM((slots, share), BF16),
            ret=pltpu.VMEM((slots, share), BF16),
            comb=pltpu.VMEM((tokens, 128), F32),
            acc=pltpu.VMEM((tokens, share), F32),
            mixed_b=pltpu.VMEM((tokens, share), BF16),
            na=pltpu.VMEM((rows_a, width), BF16),
            q=pltpu.VMEM((rows_a, qkv), BF16),
            k=pltpu.VMEM((rows_a, qkv), BF16),
            v=pltpu.VMEM((rows_a, qkv), BF16),
            gates=pltpu.VMEM((32, BLOCK), F32),
            turn=pltpu.VMEM((BLOCK, BLOCK), F32),
            turned=pltpu.VMEM((BLOCK, BLOCK), F32),
            sums=pltpu.VMEM((heads * blocks, *state), F32),
            own=pltpu.VMEM((heads, *state), F32),
            other=pltpu.VMEM((heads, *state), F32),
            start=pltpu.VMEM((heads, *state), F32),
            current=pltpu.VMEM((heads, *state), F32),
            y_in=pltpu.VMEM((ny, *state), F32),
            y_run=pltpu.VMEM((2, *state), F32),
            z_in=pltpu.VMEM((nz, *part), F32),
            z_run=pltpu.VMEM((2, *part), F32),
            line=pltpu.VMEM((ny, *part), F32),
            cell=pltpu.VMEM((nx, BLOCK, qkv), BF16),
            cells=pltpu.VMEM((nx, BLOCK, qkv), BF16),
            mixed=pltpu.VMEM((BLOCK, width), BF16),
            load_s=dma((11,)),
            kept_s=dma((2,)),
            out_s=dma((2,)),
            down_ss=dma((6,)),
            relay_rs=dma((2,)),
            far_rs=dma((2,)),
            down_rs=dma((nx,)),
            disp_ss=dma((nz,)),
            disp_rs=dma((nz,)),
            tok_ss=dma((4, nz)),
            tok_rs=dma((4, nz)),
            hid_ss=dma((4, nz)),
            hid_rs=dma((4, nz)),
            ret_ss=dma((nz,)),
            ret_rs=dma((nz,)),
            w_ss=dma((4, 1)),
            w_rs=dma((4, 1)),
            wy_ss=dma((4, nx - 1)),
            wy_rs=dma((4, nx - 1)),
            wm_ss=dma((nx,)),
            wm_rs=dma((nx,)),
            mate_ss=dma((2,)),
            mate_rs=dma((2,)),
            y_ss=dma((ny,)),
            y_rs=dma((ny,)),
            line_ss=dma((ny,)),
            line_rs=dma((ny,)),
            z_ss=dma((nz,)),
            z_rs=dma((nz,)),
            cell_ss=dma((nx,)),
            cell_rs=dma((nx,)),
        )
        names = [*inputs, "out_a", "out_b", *scratch]
        when = SimpleNamespace(
            chip=0,
            plane=2,
            weights=3,
            line=6,
            start=7,
            attend=8,
            pass_down=1,
            wout_start=1,
            wout_forward=3,
            wout_turn=4,
            wout_pass=6,
            wout_spread=9,
            mix=12,
        )
        lag = SimpleNamespace(take=0, forward=1, expand=2, hidden=3, contract=4, gather=6)
        dims = SimpleNamespace(nz=nz, ny=ny, nx=nx, near=near, names=names, when=when, lag=lag)
        return pl.pallas_call(
            functools.partial(kernel, dims),
            out_shape=(
                jax.ShapeDtypeStruct((rows_a // nx, width), BF16),
                jax.ShapeDtypeStruct((tokens, share), BF16),
            ),
            in_specs=[spec for _, spec in inputs.values()],
            out_specs=(hbm, hbm),
            scratch_shapes=list(scratch.values()),
            compiler_params=pltpu.CompilerParams(
                collective_id=0, has_side_effects=True, vmem_limit_bytes=60 * 1024 * 1024
            ),
            name="mixer_and_experts",
        )(*[value for value, _ in inputs.values()])

    placed = (
        P("ep", None),
        P(),
        P(None, "tp"),
        P(None, "tp"),
        P(None, "tp"),
        P("tp", "ep"),
        P("tp", "ep"),
        P(),
        P("tp", None),
        P("ep", None),
        P(),
        P(),
        P(),
        P("ep", None),
        P("ep", None, "tp"),
        P("ep", None, "tp"),
        P("ep", "tp", None),
    )
    return jax.shard_map(
        shards,
        mesh=mesh,
        in_specs=placed,
        out_specs=(P(("ep", "tp"), None), P("ep", "tp")),
        check_vma=False,
    )
```

time: 277 us -> 102 us (0.37)
  Pallas kernels: 0 us -> 97.1 us
  waiting for transfers between devices: 87.1 us -> 0 us
  blocking collectives: 59.3 us -> 0 us
  local copies, waits for them, and re-layouts: 34.3 us -> 3.55 us
  matrix products: 28.8 us -> 0 us
  starting transfers between devices: 25.3 us -> 0 us
  other arithmetic: 24.5 us -> 0 us
  between operations: 16.5 us -> 0.65 us
    pallas_call x0 -> x1, Pallas kernels: none -> 97.1 us  [shards(): pl.pallas_call(functools.partial(kernel, dims), out_shape=(jax.ShapeDtype...]
    all_to_all x2 -> x0, waiting for transfers between devices: 87 us -> none  [the longest x1 74.5 us: shards(): lax.all_to_all(outgoing, EP, split_axis=0, concat_axis=0, tiled=True)]
    all_to_all x1 -> x0, blocking collectives: 41.8 us -> none  [sum_at_owner(): parts = lax.all_to_all(split_up(x, dim, length), axis, 0, 0, tiled=True)]
    dot_general x11 -> x0, matrix products: 28.8 us -> none  [the longest x1 9.1 us: shards(): jnp.einsum('scf,fo->sco', hidden, down_weight, preferred_element_type=jnp...]
    all_to_all x2 -> x0, starting transfers between devices: 25.1 us -> none  [the longest x1 13.5 us: shards(): lax.all_to_all(outgoing, EP, split_axis=0, concat_axis=0, tiled=True)]
    gather x13 -> x0, local copies, waits for them, and re-layouts: 18.2 us -> none  [the longest x1 5.98 us: shards(): padded[owner // 2].reshape(expert_total, capacity, normed_b.shape[1])]
    all_gather x2 -> x0, blocking collectives: 17.5 us -> none  [collected_together(): both, at, found = (lax.all_gather(jnp.concatenate(lines), axis), 0, {})]
    reduce_sum x5 -> x0, other arithmetic: 9.55 us -> none  [the longest x2 3.59 us: rms_rows(): jnp.mean(widened * widened, axis=-1, keepdims=True) + epsilon]
  transfers between devices with their start and end apart: 4 -> 0, of which waited for: 2 -> 0; matrix products, arithmetic and copies ran while one was open for 24% -> 0% of each run, Pallas kernels for 0% -> 0%
where the time goes in v2:
time: 102 us; the launch traced here: 101 us
  Pallas kernels  97.1 us (95%)
  local copies, waits for them, and re-layouts  3.55 us (3%)
    pallas_call x1, Pallas kernels, shards(): pl.pallas_call(functools.partial(kernel, dims), out_shape=(jax.ShapeDtype...  97.1 us
    unnamed x2, local copies, waits for them, and re-layouts  3.55 us

profile of v2, /device:TPU:1, one launch (start us, length us, event | category | flops | bytes accessed | tf_op | source)
XLA Modules:
  0.0 101.3 jit_solution(13110620981959527015)
XLA Ops:
  0.6 97.1 %mixer_and_experts.1 = (bf16[128,2048]{1,0:T(8,128)(2,1)}, bf16[256,512]{1,0:T(8,128)(2,1)}) custom-call(bf16[512,2048]{1,0:T(8,128)(2,1)} %refs_0_.1, f32[1,2048]{1,0:T(1,128)} %bitcast.14, bf16[2048,256]{1,0:T(8,128)(2,1)} %refs_2_.1, bf16[2048,256]{1,0:T(8,128)(2,1)} %refs_3_.1, bf16[2048,256]{1,0:T(8,128)(2,1)} %refs_4_.1, f32[2,512]{1,0:T(2,128)} %refs_5_.1, ...), custom_call_target="tpu_custom_call" | custom-call | tf_op jit(solution)/shard_map/mixer_and_experts/pallas_call | solution.py:1006
  97.7 1.9 %copy.21 = bf16[128,2048]{1,0:T(8,128)(2,1)} copy(bf16[128,2048]{1,0:T(8,128)(2,1)} %get-tuple-element.4) | data formatting | bytes 1048576
  99.6 1.7 %copy.22 = bf16[256,512]{1,0:T(8,128)(2,1)} copy(bf16[256,512]{1,0:T(8,128)(2,1)} %get-tuple-element.5) | data formatting | bytes 524288

commit v3 on v2

--- a/solution.py
+++ b/solution.py
@@ -13,7 +13,7 @@
 BF16 = jnp.bfloat16
 BLOCK = 128
 CORES = 2
-NEAR = 2
+NEAR = 3
 EPSILON = 1e-06
 FLOOR = -1e30
 HIGHEST = lax.Precision.HIGHEST
@@ -799,7 +799,7 @@
             pl.when(i == place)(job)
         return carry
 
-    lax.fori_loop(0, max(nz + lag.gather, when.mix + 1), step, 0)
+    lax.fori_loop(min(0, lag.take), max(nz + lag.gather, when.mix + 1), step, 0)
 
     r.mixed_b[...] = r.acc[...].astype(BF16)
     last = pltpu.make_async_copy(r.mixed_b, r.out_b, r.out_s.at[1])
@@ -848,6 +848,24 @@
     settle(r.start.at[c], r.mate_ss.at[1])
     settle(r.mixed, r.out_s.at[0])
     last.wait()
+
+
+def hand_out(a, b, out_a, out_b, held_a, held_b, sems):
+    reads = [
+        pltpu.make_async_copy(a, held_a, sems.at[0]),
+        pltpu.make_async_copy(b, held_b, sems.at[1]),
+    ]
+    writes = [
+        pltpu.make_async_copy(held_a, out_a, sems.at[2]),
+        pltpu.make_async_copy(held_b, out_b, sems.at[3]),
+    ]
+    for read in reads:
+        read.start()
+    for read, write in zip(reads, writes):
+        read.wait()
+        write.start()
+    for write in writes:
+        write.wait()
 
 
 def solution(mesh, shape=(8, 4)):
@@ -991,19 +1009,19 @@
             plane=2,
             weights=3,
             line=6,
-            start=7,
-            attend=8,
+            start=8,
+            attend=9,
             pass_down=1,
             wout_start=1,
             wout_forward=3,
             wout_turn=4,
-            wout_pass=6,
+            wout_pass=7,
             wout_spread=9,
             mix=12,
         )
-        lag = SimpleNamespace(take=0, forward=1, expand=2, hidden=3, contract=4, gather=6)
+        lag = SimpleNamespace(take=0, forward=1, expand=2, hidden=3, contract=4, gather=8)
         dims = SimpleNamespace(nz=nz, ny=ny, nx=nx, near=near, names=names, when=when, lag=lag)
-        return pl.pallas_call(
+        results = pl.pallas_call(
             functools.partial(kernel, dims),
             out_shape=(
                 jax.ShapeDtypeStruct((rows_a // nx, width), BF16),
@@ -1017,6 +1035,13 @@
             ),
             name="mixer_and_experts",
         )(*[value for value, _ in inputs.values()])
+        return pl.pallas_call(
+            hand_out,
+            out_shape=[jax.ShapeDtypeStruct(part.shape, part.dtype) for part in results],
+            in_specs=[hbm, hbm],
+            out_specs=[hbm, hbm],
+            scratch_shapes=[pltpu.VMEM(part.shape, part.dtype) for part in results] + [dma((4,))],
+        )(*results)
 
     placed = (
         P("ep", None),

time: 102 us -> 92.2 us (0.904)
  Pallas kernels: 97.1 us -> 91.4 us
  local copies, waits for them, and re-layouts: 3.55 us -> 0 us
    pallas_call x1, Pallas kernels: 97.1 us -> 89.5 us  [shards(): pl.pallas_call(functools.partial(kernel, dims), out_shape=(jax.ShapeDtype...]
    unnamed x2 -> x0, local copies, waits for them, and re-layouts: 3.55 us -> none
    pallas_call x0 -> x1, Pallas kernels: none -> 1.95 us  [shards(): pl.pallas_call(hand_out, out_shape=[jax.ShapeDtypeStruct(part.shape, part...]
where the time goes in v3:
time: 92.2 us; the launch traced here: 92.1 us
  Pallas kernels  91.4 us (99%)
    pallas_call x1, Pallas kernels, shards(): pl.pallas_call(functools.partial(kernel, dims), out_shape=(jax.ShapeDtype...  89.5 us
    pallas_call x1, Pallas kernels, shards(): pl.pallas_call(hand_out, out_shape=[jax.ShapeDtypeStruct(part.shape, part...  1.95 us

profile of v3, /device:TPU:1, one launch (start us, length us, event | category | flops | bytes accessed | tf_op | source)
XLA Modules:
  0.0 92.1 jit_solution(1138599073257273608)
XLA Ops:
  0.6 89.5 %mixer_and_experts.1 = (bf16[128,2048]{1,0:T(8,128)(2,1)}, bf16[256,512]{1,0:T(8,128)(2,1)}) custom-call(bf16[512,2048]{1,0:T(8,128)(2,1)} %refs_0_.1, f32[1,2048]{1,0:T(1,128)} %bitcast.14, bf16[2048,256]{1,0:T(8,128)(2,1)} %refs_2_.1, bf16[2048,256]{1,0:T(8,128)(2,1)} %refs_3_.1, bf16[2048,256]{1,0:T(8,128)(2,1)} %refs_4_.1, f32[2,512]{1,0:T(2,128)} %refs_5_.1, ...), custom_call_target="tpu_custom_call" | custom-call | tf_op jit(solution)/shard_map/mixer_and_experts/pallas_call | solution.py:1024
  90.1 2.0 %shard_map.176 = (bf16[128,2048]{1,0:T(8,128)(2,1)}, bf16[256,512]{1,0:T(8,128)(2,1)}) custom-call(bf16[128,2048]{1,0:T(8,128)(2,1)} %get-tuple-element.4.a, bf16[256,512]{1,0:T(8,128)(2,1)} %get-tuple-element.5.b), custom_call_target="tpu_custom_call" | custom-call | tf_op jit(solution)/shard_map/pallas_call | solution.py:1038
